TPU v7x, 32 devices: a whole 2x2x4 slice. The times are simulated.
32 devices in a mesh: sp: 8 (over z, x), tp: 4 (over y, core).
Axes of the slice: x: 2, y: 2, z: 4, core: 2. Of those that a mesh axis runs over, the one named last changes fastest.
Arguments:
- layer_input: bfloat16 [1280, 4096], P('sp', 'tp'), may hold values from -24 to 24
- output_grad: bfloat16 [1280, 4096], P('sp', 'tp'), may hold values from -24 to 24
- query_weight: bfloat16 [4096, 2048], P(None, 'tp'), may hold values from -0.09375 to 0.09375
- key_weight: bfloat16 [4096, 1024], P(None, 'tp'), may hold values from -0.09375 to 0.09375
- value_weight: bfloat16 [4096, 1024], P(None, 'tp'), may hold values from -0.09375 to 0.09375
- out_weight: bfloat16 [2048, 4096], P('tp'), may hold values from -0.125 to 0.125
- sink_logit: float32 [16], P('tp'), may hold values from 3 to 7
Outputs:
- input_grad: bfloat16 [1280, 4096], P('sp', 'tp')
- query_weight_grad: float32 [4096, 2048], P('sp', 'tp')
- key_weight_grad: float32 [4096, 1024], P('sp', 'tp')
- value_weight_grad: float32 [4096, 1024], P('sp', 'tp')
- out_weight_grad: float32 [2048, 4096], P('tp', 'sp')
- sink_grad: float32 [16], P('tp')
All inputs are finite; a program needn't handle non-finite values.
Results may differ from a plain program's by a relative error of at most 0.015.
Values may be sent and summed in bfloat16 or wider, within the bound.
A program may use at most 192 MiB of HBM per device.

v0:
```python
import functools

import jax
import jax.numpy as jnp
from jax import lax
from jax.experimental import pallas as pl
from jax.experimental.pallas import tpu as pltpu
from jax.sharding import PartitionSpec as P

HEADS = 16
KV_HEADS = 8
HEAD = 128
WINDOW = 128


masked_score = -1e30


def extended(cells, sides, width):
    for axis, dim in sides:
        count = lax.axis_size(axis)
        ends = count - 1
        head = lax.slice_in_dim(cells, 0, width, axis=dim)
        tail = lax.slice_in_dim(cells, cells.shape[dim] - width, cells.shape[dim], axis=dim)
        cells = jnp.concatenate(
            [
                lax.ppermute(tail, axis, [(i, (i + 1) % count) for i in range(ends)]),
                cells,
                lax.ppermute(head, axis, [((i + 1) % count, i) for i in range(ends)]),
            ],
            axis=dim,
        )
    return cells


def passed_along(value, axis, steps):
    count = lax.axis_size(axis)
    initial, last = (max(0, -steps), min(count, count - steps))
    return lax.ppermute(value, axis, [(source, source + steps) for source in range(initial, last)])


def contract_rows(left, right):
    return lax.dot_general(
        left, right, (((0,), (0,)), ((), ())), preferred_element_type=jnp.float32
    )


def contract_cols(left, right):
    return lax.dot_general(
        left, right, (((1,), (1,)), ((), ())), preferred_element_type=jnp.float32
    )


def per_device(
    layer_input, output_grad, query_weight, key_weight, value_weight, out_weight, sink_logit
):
    whole_input, whole_grad = (
        lax.all_gather(layer_input, "tp", axis=1, tiled=True),
        lax.all_gather(output_grad, "tp", axis=1, tiled=True),
    )
    tok_rows = whole_input.shape[0]
    query_cols = query_weight.shape[1]
    key_cols = key_weight.shape[1]
    key_heads = key_cols // HEAD
    group_size = HEADS // KV_HEADS
    scaling = HEAD ** (-0.5)
    queries = jnp.dot(whole_input, query_weight, preferred_element_type=jnp.float32).astype(
        jnp.bfloat16
    )
    key_rows = jnp.dot(whole_input, key_weight, preferred_element_type=jnp.float32).astype(
        jnp.bfloat16
    )
    value_rows = jnp.dot(whole_input, value_weight, preferred_element_type=jnp.float32).astype(
        jnp.bfloat16
    )
    out_rows_grad = contract_cols(whole_grad, out_weight).astype(jnp.bfloat16)
    joined = jnp.concatenate([key_rows, value_rows], axis=1)
    band = extended(joined, (("sp", 0),), WINDOW)
    band_rows = band.shape[0]
    band_keys = band[:, :key_cols].reshape(band_rows, key_heads, HEAD)
    band_values = band[:, key_cols:].reshape(band_rows, key_heads, HEAD)
    shard_index = lax.axis_index("sp")
    seq_total = tok_rows * lax.axis_size("sp")
    query_pos = shard_index * tok_rows + jnp.arange(tok_rows, dtype=jnp.int32)
    key_pos = shard_index * tok_rows - WINDOW + jnp.arange(band_rows, dtype=jnp.int32)
    in_window = (
        (jnp.abs(query_pos[:, None] - key_pos[None, :]) <= WINDOW)
        & (key_pos[None, :] >= 0)
        & (key_pos[None, :] < seq_total)
    )
    query_heads = queries.reshape(tok_rows, key_heads, group_size, HEAD)
    grad_heads = out_rows_grad.reshape(tok_rows, key_heads, group_size, HEAD)
    scores = (
        jnp.einsum("qkgd,skd->kgqs", query_heads, band_keys, preferred_element_type=jnp.float32)
        * scaling
    )
    scores = jnp.where(in_window[None, None], scores, masked_score)
    sink_column = sink_logit.reshape(key_heads, group_size)[:, :, None]
    row_max = jnp.maximum(jnp.max(scores, axis=-1), sink_column)
    row_total = jnp.sum(jnp.exp(scores - row_max[..., None]), axis=-1) + jnp.exp(
        sink_column - row_max
    )
    log_total = row_max + jnp.log(row_total)
    soft_weights = jnp.exp(scores - log_total[..., None])
    soft_rounded = soft_weights.astype(jnp.bfloat16)
    attended = jnp.einsum(
        "kgqs,skd->qkgd", soft_rounded, band_values, preferred_element_type=jnp.float32
    ).astype(jnp.bfloat16)
    row_dots = jnp.sum(
        grad_heads.astype(jnp.float32) * attended.astype(jnp.float32), axis=-1
    ).transpose(1, 2, 0)
    prob_grads = jnp.einsum(
        "qkgd,skd->kgqs", grad_heads, band_values, preferred_element_type=jnp.float32
    )
    score_grads = (soft_weights * (prob_grads - row_dots[..., None])).astype(jnp.bfloat16)
    query_grads = (
        jnp.einsum("kgqs,skd->qkgd", score_grads, band_keys, preferred_element_type=jnp.float32)
        * scaling
    )
    query_grads = query_grads.astype(jnp.bfloat16).reshape(tok_rows, query_cols)
    band_key_grads = (
        jnp.einsum("kgqs,qkgd->skd", score_grads, query_heads, preferred_element_type=jnp.float32)
        * scaling
    )
    band_value_grads = jnp.einsum(
        "kgqs,qkgd->skd", soft_rounded, grad_heads, preferred_element_type=jnp.float32
    )
    band_grads = jnp.concatenate(
        [
            band_key_grads.reshape(band_rows, key_cols),
            band_value_grads.reshape(band_rows, key_cols),
        ],
        axis=1,
    )
    sink_part = -jnp.sum(jnp.exp(sink_column - log_total) * row_dots, axis=-1).reshape(-1)
    sink_grad = lax.psum(sink_part, "sp")
    attended_rows = attended.reshape(tok_rows, query_cols)
    input_block = lax.all_to_all(whole_input, "sp", 1, 0, tiled=True)
    grad_block = lax.all_to_all(whole_grad, "sp", 1, 0, tiled=True)
    early_rows = lax.all_gather(
        jnp.concatenate([query_grads, attended_rows], axis=1), "sp", axis=0, tiled=True
    )
    query_part = contract_rows(input_block, early_rows[:, :query_cols])
    out_part = contract_rows(early_rows[:, query_cols:], grad_block)
    returned_low = passed_along(band_grads[:WINDOW].astype(jnp.bfloat16), "sp", -1).astype(
        jnp.float32
    )
    returned_high = passed_along(
        band_grads[band_rows - WINDOW :].astype(jnp.bfloat16), "sp", 1
    ).astype(jnp.float32)
    own_rows = band_grads[WINDOW : WINDOW + tok_rows]
    own_rows = own_rows.at[tok_rows - WINDOW :].add(returned_low)
    own_rows = own_rows.at[:WINDOW].add(returned_high)
    key_grads = own_rows[:, :key_cols].astype(jnp.bfloat16)
    value_grads = own_rows[:, key_cols:].astype(jnp.bfloat16)
    late_rows = lax.all_gather(
        jnp.concatenate([key_grads, value_grads], axis=1), "sp", axis=0, tiled=True
    )
    key_part = contract_rows(input_block, late_rows[:, :key_cols])
    value_part = contract_rows(input_block, late_rows[:, key_cols:])
    partials = (
        contract_cols(query_grads, query_weight)
        + contract_cols(key_grads, key_weight)
        + contract_cols(value_grads, value_weight)
    )
    input_grad = lax.psum_scatter(
        partials.astype(jnp.bfloat16), "tp", scatter_dimension=1, tiled=True
    )
    return (input_grad, query_part, key_part, value_part, out_part, sink_grad)


LANES = 128
MESH = pl.DeviceIdType.MESH
VMEM_BYTES = 60 * 1024 * 1024


def dot_nn(a, b):
    return jnp.dot(a, b, preferred_element_type=jnp.float32)


def layer_kernel(
    x_ref, g_ref, wq_hbm, wk_hbm, wv_hbm, wo_hbm, sink_ref,
    ig_ref, gq_ref, gk_ref, gv_ref, go_ref, sg_ref,
    wq, wk, wv, wo, xg, acc, qs, dos, band, bg, ret_out, ret_in,
    blk, acts_e, acts_l, part, rs_in, sinks,
    w_sem, own_sem, ag_send, ag_recv, halo_send, halo_recv, ret_send, ret_recv,
    a2a_send, a2a_recv, blk_send, blk_recv, up_sem, down_sem, cross_sem, acts_recv,
    rs_send, rs_recv, sink_send, sink_recv,
):
    bf16 = jnp.bfloat16
    count, tps = lax.axis_size("sp"), lax.axis_size("tp")
    depth = count // 2
    s, t = lax.axis_index("sp"), lax.axis_index("tp")
    z, x = s // 2, s % 2
    y, core = t // 2, t % 2
    partner = y * 2 + (1 - core)
    across = (1 - y) * 2 + core
    diag = (1 - y) * 2 + (1 - core)
    rows, feats = x_ref.shape
    q_cols, k_cols = wq.shape[1], wk.shape[1]
    block_cols = gq_ref.shape[0]
    per_slot = feats // block_cols
    key_heads = k_cols // HEAD
    group = q_cols // k_cols
    scaling = HEAD**-0.5

    def remote(src, dst, send, recv, dev_s, dev_t):
        return pltpu.make_async_remote_copy(
            src_ref=src, dst_ref=dst, send_sem=send, recv_sem=recv,
            device_id=(dev_s, dev_t), device_id_type=MESH,
        )

    weights = [
        pltpu.make_async_copy(src, dst, w_sem.at[i])
        for i, (src, dst) in enumerate(((wq_hbm, wq), (wk_hbm, wk), (wv_hbm, wv), (wo_hbm, wo)))
    ]
    for copy in weights:
        copy.start()
    own = [
        pltpu.make_async_copy(ref, xg.at[t, a], own_sem.at[a])
        for a, ref in enumerate((x_ref, g_ref))
    ]
    for copy in own:
        copy.start()

    barrier = pltpu.get_barrier_semaphore()
    for peer in (partner, across, diag):
        pl.semaphore_signal(barrier, inc=1, device_id=(s, peer), device_id_type=MESH)
    for d in range(1, count):
        pl.semaphore_signal(
            barrier, inc=1, device_id=((s + d) % count, t), device_id_type=MESH
        )
    pl.semaphore_wait(barrier, 3 + count - 1)

    sources = (x_ref, g_ref)
    to_across = [
        remote(sources[a], xg.at[t, a], ag_send.at[0, a], ag_recv.at[0, a], s, across)
        for a in range(2)
    ]
    to_partner = [
        remote(sources[a], xg.at[t, a], ag_send.at[1, a], ag_recv.at[1, a], s, partner)
        for a in range(2)
    ]
    relay = [
        remote(xg.at[across, a], xg.at[across, a], ag_send.at[2, a], ag_recv.at[2, a], s, partner)
        for a in range(2)
    ]
    for copy in to_across + to_partner:
        copy.start()

    def project_input(slot, first):
        cells = xg[slot, 0]
        span = pl.ds(pl.multiple_of(slot * feats, feats), feats)
        at = 0
        for w in (wq, wk, wv):
            cols = w.shape[1]
            term = dot_nn(cells, w[span, :])
            acc[:, at : at + cols] = term if first else acc[:, at : at + cols] + term
            at += cols

    def project_grad(slot, first):
        span = pl.ds(pl.multiple_of(slot * feats, feats), feats)
        term = contract_cols(xg[slot, 1], wo[:, span])
        lo = q_cols + 2 * k_cols
        acc[:, lo:] = term if first else acc[:, lo:] + term

    for copy in own + weights:
        copy.wait()
    project_input(t, True)
    project_grad(t, True)
    to_partner[0].wait_recv()
    project_input(partner, False)
    to_partner[1].wait_recv()
    project_grad(partner, False)
    to_across[0].wait_recv()
    relay[0].start()
    project_input(across, False)
    relay[0].wait_recv()
    project_input(diag, False)

    mid = pl.ds(WINDOW, rows)
    band[mid, :] = acc[:, q_cols : q_cols + 2 * k_cols].astype(bf16)
    qs[...] = acc[:, :q_cols].astype(bf16)
    has_prev, has_next = s > 0, s < count - 1
    prev, nxt = lax.rem(s + count - 1, count), lax.rem(s + 1, count)
    low, high = pl.ds(0, WINDOW), pl.ds(WINDOW + rows, WINDOW)
    tail_copy = remote(
        band.at[pl.ds(rows, WINDOW)], band.at[low], halo_send.at[0], halo_recv.at[0], nxt, t
    )
    head_copy = remote(
        band.at[pl.ds(WINDOW, WINDOW)], band.at[high], halo_send.at[1], halo_recv.at[1], prev, t
    )

    @pl.when(has_next)
    def _():
        tail_copy.start()

    @pl.when(has_prev)
    def _():
        head_copy.start()

    own_blocks, a2a = [], []

    def columns(a, j):
        lane = (j % per_slot) * block_cols + t * LANES
        return xg.at[j // per_slot, a, :, pl.ds(pl.multiple_of(lane, LANES), LANES)]

    def send_columns(a):
        own_blocks.append(
            pltpu.make_async_copy(columns(a, s), blk.at[t, s, a], own_sem.at[2 + a])
        )
        own_blocks[-1].start()
        for d in range(1, count):
            j = (s + d) % count
            a2a.append(
                remote(
                    columns(a, j), blk.at[t, s, a], a2a_send.at[a, d], a2a_recv.at[a, d], j, t
                )
            )
            a2a[-1].start()

    send_columns(0)
    to_across[1].wait_recv()
    relay[1].start()
    project_grad(across, False)
    relay[1].wait_recv()
    project_grad(diag, False)
    dos[...] = acc[:, q_cols + 2 * k_cols :].astype(bf16)

    send_columns(1)

    @pl.when(jnp.logical_not(has_prev))
    def _():
        band[low, :] = jnp.zeros((WINDOW, 2 * k_cols), bf16)

    @pl.when(jnp.logical_not(has_next))
    def _():
        band[high, :] = jnp.zeros((WINDOW, 2 * k_cols), bf16)

    @pl.when(has_prev)
    def _():
        tail_copy.wait_recv()

    @pl.when(has_next)
    def _():
        head_copy.wait_recv()

    band_rows = rows + 2 * WINDOW
    q_at = lax.broadcasted_iota(jnp.int32, (rows, band_rows), 0)
    k_at = lax.broadcasted_iota(jnp.int32, (rows, band_rows), 1) - WINDOW
    k_pos = k_at + s * rows
    in_window = (
        (jnp.abs(q_at - k_at) <= WINDOW) & (k_pos >= 0) & (k_pos < rows * count)
    )
    lane_at = lax.broadcasted_iota(jnp.int32, (8, LANES), 1)
    sink_row = jnp.zeros((8, LANES), jnp.float32)
    for kh in range(key_heads):
        keys = band[:, kh * HEAD : (kh + 1) * HEAD]
        values = band[:, k_cols + kh * HEAD : k_cols + (kh + 1) * HEAD]
        key_sum = value_sum = None
        for g in range(group):
            h = kh * group + g
            cols = slice(h * HEAD, (h + 1) * HEAD)
            q, do = qs[:, cols], dos[:, cols]
            scores = jnp.where(in_window, contract_cols(q, keys) * scaling, masked_score)
            sink = sink_ref[0, h]
            top = jnp.maximum(jnp.max(scores, axis=1, keepdims=True), sink)
            e = jnp.exp(scores - top)
            sink_e = jnp.exp(sink - top)
            inverse = 1.0 / (jnp.sum(e, axis=1, keepdims=True) + sink_e)
            p = e * inverse
            p_low = p.astype(bf16)
            attended = dot_nn(p_low, values).astype(bf16)
            dots = jnp.sum(
                do.astype(jnp.float32) * attended.astype(jnp.float32), axis=1, keepdims=True
            )
            ds = (p * (contract_cols(do, values) - dots)).astype(bf16)
            acts_e[s, :, cols] = (dot_nn(ds, keys) * scaling).astype(bf16)
            acts_e[s, :, q_cols + h * HEAD : q_cols + (h + 1) * HEAD] = attended
            kg, vg = contract_rows(ds, q), contract_rows(p_low, do)
            key_sum = kg if g == 0 else key_sum + kg
            value_sum = vg if g == 0 else value_sum + vg
            total = -jnp.sum(sink_e * inverse * dots)
            sink_row = jnp.where(lane_at == h, total, sink_row)
        bg[:, kh * HEAD : (kh + 1) * HEAD] = key_sum * scaling
        bg[:, k_cols + kh * HEAD : k_cols + (kh + 1) * HEAD] = value_sum
    sinks[s] = sink_row
    ret_out[0] = bg[low, :].astype(bf16)
    ret_out[1] = bg[high, :].astype(bf16)
    to_prev = remote(ret_out.at[0], ret_in.at[0], ret_send.at[0], ret_recv.at[0], prev, t)
    to_next = remote(ret_out.at[1], ret_in.at[1], ret_send.at[1], ret_recv.at[1], nxt, t)

    @pl.when(has_prev)
    def _():
        to_prev.start()

    @pl.when(has_next)
    def _():
        to_next.start()

    acts = (acts_e, acts_l)
    has_up, has_down = z < depth - 1, z > 0
    up, down, other = (z + 1) % depth * 2 + x, (z + depth - 1) % depth * 2 + x, z * 2 + (1 - x)

    def acts_copy(a, block, sems, dev):
        ref = acts[a].at[block]
        return remote(ref, ref, sems.at[a, block], acts_recv.at[a, block], dev, t)

    def send_own(a):
        acts_copy(a, s, cross_sem, other).start()

        @pl.when(has_up)
        def _():
            acts_copy(a, s, up_sem, up).start()

        @pl.when(has_down)
        def _():
            acts_copy(a, s, down_sem, down).start()

    send_own(0)
    sink_copies = []
    for d in range(1, count):
        sink_copies.append(
            remote(
                sinks.at[s], sinks.at[s], sink_send.at[d], sink_recv.at[d], (s + d) % count, t
            )
        )
        sink_copies[-1].start()

    tail, head = pl.ds(WINDOW + rows - WINDOW, WINDOW), pl.ds(WINDOW, WINDOW)

    @pl.when(has_next)
    def _():
        to_prev.wait_recv()
        bg[tail, :] = bg[tail, :] + ret_in[0].astype(jnp.float32)

    @pl.when(has_prev)
    def _():
        to_next.wait_recv()
        bg[head, :] = bg[head, :] + ret_in[1].astype(jnp.float32)

    acts_l[s] = bg[mid, :].astype(bf16)
    send_own(1)

    for copy in own_blocks:
        copy.wait()
    for copy in a2a:
        copy.wait_recv()
    blk_across = remote(blk.at[t], blk.at[t], blk_send.at[0], blk_recv.at[0], s, across)
    blk_partner = remote(blk.at[t], blk.at[t], blk_send.at[1], blk_recv.at[1], s, partner)
    blk_relay = remote(blk.at[across], blk.at[across], blk_send.at[2], blk_recv.at[2], s, partner)
    blk_across.start()
    blk_partner.start()
    qg = acts_e[s, :, :q_cols]
    kg, vg = acts_l[s, :, :k_cols], acts_l[s, :, k_cols:]

    def partial_for(slot):
        span = pl.ds(pl.multiple_of(slot * feats, feats), feats)
        return (
            contract_cols(qg, wq[span, :])
            + contract_cols(kg, wk[span, :])
            + contract_cols(vg, wv[span, :])
        ).astype(bf16)

    rs_copies = []
    for i, peer in enumerate((across, diag, partner)):
        part[i] = partial_for(peer)
        rs_copies.append(
            remote(part.at[i], rs_in.at[i], rs_send.at[i], rs_recv.at[i], s, peer)
        )
        rs_copies[-1].start()

    def forward(d):
        for a in range(2):
            lower, upper = (z + depth - d) % depth * 2 + x, (z + d) % depth * 2 + x

            @pl.when(z >= d)
            def _():
                acts_copy(a, lower, up_sem, up).wait_recv()
                acts_copy(a, lower, cross_sem, other).start()

                @pl.when(has_up)
                def _():
                    acts_copy(a, lower, up_sem, up).start()

            @pl.when(z + d < depth)
            def _():
                acts_copy(a, upper, down_sem, down).wait_recv()
                acts_copy(a, upper, cross_sem, other).start()

                @pl.when(has_down)
                def _():
                    acts_copy(a, upper, down_sem, down).start()

    def consume(block, first=False):
        early, late = acts_e[block], acts_l[block]
        right = jnp.concatenate([early[:, :q_cols], late], axis=1)
        left = jnp.concatenate([blk[i, block, 0] for i in range(tps)], axis=1)
        grads = jnp.concatenate([blk[i, block, 1] for i in range(tps)], axis=1)
        term = contract_rows(left, right)
        out_term = contract_rows(early[:, q_cols:], grads)
        pieces = (
            (gq_ref, term[:, :q_cols]),
            (gk_ref, term[:, q_cols : q_cols + k_cols]),
            (gv_ref, term[:, q_cols + k_cols :]),
            (go_ref, out_term),
        )
        for ref, value in pieces:
            ref[...] = value if first else ref[...] + value

    def consume_crossed(block_z):
        block = block_z * 2 + (1 - x)
        for a in range(2):
            acts_copy(a, block, cross_sem, other).wait_recv()
        consume(block)

    def consume_far(d):
        lower, upper = (z + depth - d) % depth, (z + d) % depth

        @pl.when(z >= d)
        def _():
            consume(lower * 2 + x)
            consume_crossed(lower)

        @pl.when(z + d < depth)
        def _():
            consume(upper * 2 + x)
            consume_crossed(upper)

    mine = partial_for(t)
    forward(1)
    blk_across.wait_recv()
    blk_relay.start()
    for d in range(2, depth):
        forward(d)
    blk_partner.wait_recv()
    blk_relay.wait_recv()
    consume(s, True)
    consume_crossed(z)
    for d in range(1, depth):
        consume_far(d)
    for copy in rs_copies:
        copy.wait_recv()
    total = mine.astype(jnp.float32)
    for i in range(3):
        total = total + rs_in[i].astype(jnp.float32)
    ig_ref[...] = total.astype(bf16)
    for copy in sink_copies:
        copy.wait_recv()
    sink_total = sinks[0]
    for i in range(1, count):
        sink_total = sink_total + sinks[i]
    sg_ref[...] = sink_total

    for copy in to_across + to_partner + relay + a2a + rs_copies + sink_copies:
        copy.wait_send()
    for copy in (blk_across, blk_partner, blk_relay):
        copy.wait_send()

    @pl.when(has_next)
    def _():
        tail_copy.wait_send()
        to_next.wait_send()

    @pl.when(has_prev)
    def _():
        head_copy.wait_send()
        to_prev.wait_send()

    for a in range(2):
        acts_copy(a, s, cross_sem, other).wait_send()

        @pl.when(has_up)
        def _():
            acts_copy(a, s, up_sem, up).wait_send()

        @pl.when(has_down)
        def _():
            acts_copy(a, s, down_sem, down).wait_send()

        for d in range(1, depth):
            lower, upper = (z + depth - d) % depth * 2 + x, (z + d) % depth * 2 + x

            @pl.when(z >= d)
            def _():
                acts_copy(a, lower, cross_sem, other).wait_send()

                @pl.when(has_up)
                def _():
                    acts_copy(a, lower, up_sem, up).wait_send()

            @pl.when(z + d < depth)
            def _():
                acts_copy(a, upper, cross_sem, other).wait_send()

                @pl.when(has_down)
                def _():
                    acts_copy(a, upper, down_sem, down).wait_send()


def store_kernel(*refs):
    ins, sink_in, outs, sink_out = refs[:5], refs[5], refs[6:11], refs[11]
    held, in_sem, out_sem = refs[12:17], refs[17], refs[18]
    loads = [pltpu.make_async_copy(ins[i], held[i], in_sem.at[i]) for i in range(5)]
    stores = [pltpu.make_async_copy(held[i], outs[i], out_sem.at[i]) for i in range(5)]
    for load in loads:
        load.start()
    sink_out[...] = sink_in[0:1, : sink_out.shape[1]]
    for load, store in zip(loads, stores):
        load.wait()
        store.start()
    for store in stores:
        store.wait()


def fused_device(
    layer_input, output_grad, query_weight, key_weight, value_weight, out_weight, sink_logit
):
    bf16, f32 = jnp.bfloat16, jnp.float32
    count, tps = lax.axis_size("sp"), lax.axis_size("tp")
    rows, feats = layer_input.shape
    width = query_weight.shape[0]
    q_cols, k_cols = query_weight.shape[1], key_weight.shape[1]
    block_cols = width // count
    vmem = pl.BlockSpec(memory_space=pltpu.VMEM)
    hbm = pl.BlockSpec(memory_space=pl.ANY)
    dma = pltpu.SemaphoreType.DMA
    outs = pl.pallas_call(
        layer_kernel,
        out_shape=(
            jax.ShapeDtypeStruct((rows, feats), bf16),
            jax.ShapeDtypeStruct((block_cols, q_cols), f32),
            jax.ShapeDtypeStruct((block_cols, k_cols), f32),
            jax.ShapeDtypeStruct((block_cols, k_cols), f32),
            jax.ShapeDtypeStruct((q_cols, block_cols), f32),
            jax.ShapeDtypeStruct((8, LANES), f32),
        ),
        in_specs=[vmem, vmem, hbm, hbm, hbm, hbm, pl.BlockSpec(memory_space=pltpu.SMEM)],
        out_specs=(vmem,) * 6,
        scratch_shapes=[
            pltpu.VMEM(query_weight.shape, bf16),
            pltpu.VMEM(key_weight.shape, bf16),
            pltpu.VMEM(value_weight.shape, bf16),
            pltpu.VMEM(out_weight.shape, bf16),
            pltpu.VMEM((tps, 2, rows, feats), bf16),
            pltpu.VMEM((rows, 2 * q_cols + 2 * k_cols), f32),
            pltpu.VMEM((rows, q_cols), bf16),
            pltpu.VMEM((rows, q_cols), bf16),
            pltpu.VMEM((rows + 2 * WINDOW, 2 * k_cols), bf16),
            pltpu.VMEM((rows + 2 * WINDOW, 2 * k_cols), f32),
            pltpu.VMEM((2, WINDOW, 2 * k_cols), bf16),
            pltpu.VMEM((2, WINDOW, 2 * k_cols), bf16),
            pltpu.VMEM((tps, count, 2, rows, LANES), bf16),
            pltpu.VMEM((count, rows, 2 * q_cols), bf16),
            pltpu.VMEM((count, rows, 2 * k_cols), bf16),
            pltpu.VMEM((3, rows, feats), bf16),
            pltpu.VMEM((3, rows, feats), bf16),
            pltpu.VMEM((count, 8, LANES), f32),
            dma((4,)), dma((4,)), dma((3, 2)), dma((3, 2)),
            dma((2,)), dma((2,)), dma((2,)), dma((2,)),
            dma((2, count)), dma((2, count)), dma((3,)), dma((3,)),
            dma((2, count)), dma((2, count)), dma((2, count)), dma((2, count)),
            dma((3,)), dma((3,)), dma((count,)), dma((count,)),
        ],
        compiler_params=pltpu.CompilerParams(
            collective_id=0, has_side_effects=True, vmem_limit_bytes=VMEM_BYTES
        ),
        name="layer",
    )(
        layer_input, output_grad, query_weight, key_weight, value_weight, out_weight,
        sink_logit.reshape(1, -1),
    )
    kept = [jax.ShapeDtypeStruct(out.shape, out.dtype) for out in outs[:5]]
    stored = pl.pallas_call(
        store_kernel,
        out_shape=(*kept, jax.ShapeDtypeStruct((1, sink_logit.shape[0]), f32)),
        in_specs=[hbm] * 5 + [vmem],
        out_specs=(hbm,) * 5 + (vmem,),
        scratch_shapes=[pltpu.VMEM(out.shape, out.dtype) for out in kept]
        + [dma((5,)), dma((5,))],
        compiler_params=pltpu.CompilerParams(vmem_limit_bytes=VMEM_BYTES),
        name="store",
    )(*outs)
    return tuple(stored[:5]) + (stored[5].reshape(-1),)


def fits_kernel(mesh, layer_width):
    count, tps = mesh.shape["sp"], mesh.shape["tp"]
    return tps == 4 and count % 8 == 0 and layer_width == count * tps * LANES


def solution(mesh):
    placed = (
        P("sp", "tp"),
        P("sp", "tp"),
        P(None, "tp"),
        P(None, "tp"),
        P(None, "tp"),
        P("tp", None),
        P("tp"),
    )

    def sharded(*arrays):
        width = arrays[0].shape[1]
        body = fused_device if fits_kernel(mesh, width) else per_device
        return jax.shard_map(
            body,
            mesh=mesh,
            in_specs=placed,
            out_specs=(
                P("sp", "tp"),
                P("sp", "tp"),
                P("sp", "tp"),
                P("sp", "tp"),
                P("tp", "sp"),
                P("tp"),
            ),
            check_vma=False,
        )(*arrays)

    return sharded
```

profile of v0, /device:TPU:0, one launch (start us, length us, event | category | flops | bytes accessed | tf_op | source)
XLA Modules:
  0.0 88.3 jit_solution(10444675239751622547)
XLA Ops:
  0.6 83.2 %layer.1 = (bf16[160,1024]{1,0:T(8,128)(2,1)}, f32[512,512]{1,0:T(8,128)}, f32[512,256]{1,0:T(8,128)}, f32[512,256]{1,0:T(8,128)}, f32[512,512]{1,0:T(8,128)}, /*index=5*/f32[8,128]{1,0:T(8,128)}) custom-call(bf16[160,1024]{1,0:T(8,128)(2,1)} %x_ref.1, bf16[160,1024]{1,0:T(8,128)(2,1)} %g_ref.1, bf16[4096,512]{1,0:T(8,128)(2,1)} %wq_hbm.1, ...), custom_call_target="tpu_custom_call" | custom-call | tf_op jit(solution)/shard_map/layer/pallas_call | solution.py:628
  83.8 4.3 %store.1 = (bf16[160,1024]{1,0:T(8,128)(2,1)}, f32[512,512]{1,0:T(8,128)}, f32[512,256]{1,0:T(8,128)}, f32[512,256]{1,0:T(8,128)}, f32[512,512]{1,0:T(8,128)}, /*index=5*/f32[1,4]{1,0:T(1,128)}) custom-call(bf16[160,1024]{1,0:T(8,128)(2,1)} %get-tuple-element.18.refs_0_, f32[512,512]{1,0:T(8,128)} %get-tuple-element.19.refs_1_, ...), custom_call_target="tpu_custom_call" | custom-call | tf_op jit(solution)/shard_map/store/pallas_call | solution.py:674
where the time goes:
time: 89.9 us; the launch traced here: 88.3 us
  Pallas kernels  87.5 us (97%)
    pallas_call x1, Pallas kernels, fused_device(): pl.pallas_call(layer_kernel, out_shape=(jax.ShapeDtypeStruct((rows, feats...  83.2 us
    pallas_call x1, Pallas kernels, fused_device(): pl.pallas_call(store_kernel, out_shape=(*kept, jax.ShapeDtypeStruct((1, s...  4.33 us

commit v1 on v0

v1 whole, which is shorter than its diff:
```python
import functools

import jax
import jax.numpy as jnp
from jax import lax
from jax.experimental import pallas as pl
from jax.experimental.pallas import tpu as pltpu
from jax.sharding import PartitionSpec as P

HEADS = 16
KV_HEADS = 8
HEAD = 128
WINDOW = 128


masked_score = -1e30


def extended(cells, sides, width):
    for axis, dim in sides:
        count = lax.axis_size(axis)
        ends = count - 1
        head = lax.slice_in_dim(cells, 0, width, axis=dim)
        tail = lax.slice_in_dim(cells, cells.shape[dim] - width, cells.shape[dim], axis=dim)
        cells = jnp.concatenate(
            [
                lax.ppermute(tail, axis, [(i, (i + 1) % count) for i in range(ends)]),
                cells,
                lax.ppermute(head, axis, [((i + 1) % count, i) for i in range(ends)]),
            ],
            axis=dim,
        )
    return cells


def passed_along(value, axis, steps):
    count = lax.axis_size(axis)
    initial, last = (max(0, -steps), min(count, count - steps))
    return lax.ppermute(value, axis, [(source, source + steps) for source in range(initial, last)])


def contract_rows(left, right):
    return lax.dot_general(
        left, right, (((0,), (0,)), ((), ())), preferred_element_type=jnp.float32
    )


def contract_cols(left, right):
    return lax.dot_general(
        left, right, (((1,), (1,)), ((), ())), preferred_element_type=jnp.float32
    )


def per_device(
    layer_input, output_grad, query_weight, key_weight, value_weight, out_weight, sink_logit
):
    whole_input, whole_grad = (
        lax.all_gather(layer_input, "tp", axis=1, tiled=True),
        lax.all_gather(output_grad, "tp", axis=1, tiled=True),
    )
    tok_rows = whole_input.shape[0]
    query_cols = query_weight.shape[1]
    key_cols = key_weight.shape[1]
    key_heads = key_cols // HEAD
    group_size = HEADS // KV_HEADS
    scaling = HEAD ** (-0.5)
    queries = jnp.dot(whole_input, query_weight, preferred_element_type=jnp.float32).astype(
        jnp.bfloat16
    )
    key_rows = jnp.dot(whole_input, key_weight, preferred_element_type=jnp.float32).astype(
        jnp.bfloat16
    )
    value_rows = jnp.dot(whole_input, value_weight, preferred_element_type=jnp.float32).astype(
        jnp.bfloat16
    )
    out_rows_grad = contract_cols(whole_grad, out_weight).astype(jnp.bfloat16)
    joined = jnp.concatenate([key_rows, value_rows], axis=1)
    band = extended(joined, (("sp", 0),), WINDOW)
    band_rows = band.shape[0]
    band_keys = band[:, :key_cols].reshape(band_rows, key_heads, HEAD)
    band_values = band[:, key_cols:].reshape(band_rows, key_heads, HEAD)
    shard_index = lax.axis_index("sp")
    seq_total = tok_rows * lax.axis_size("sp")
    query_pos = shard_index * tok_rows + jnp.arange(tok_rows, dtype=jnp.int32)
    key_pos = shard_index * tok_rows - WINDOW + jnp.arange(band_rows, dtype=jnp.int32)
    in_window = (
        (jnp.abs(query_pos[:, None] - key_pos[None, :]) <= WINDOW)
        & (key_pos[None, :] >= 0)
        & (key_pos[None, :] < seq_total)
    )
    query_heads = queries.reshape(tok_rows, key_heads, group_size, HEAD)
    grad_heads = out_rows_grad.reshape(tok_rows, key_heads, group_size, HEAD)
    scores = (
        jnp.einsum("qkgd,skd->kgqs", query_heads, band_keys, preferred_element_type=jnp.float32)
        * scaling
    )
    scores = jnp.where(in_window[None, None], scores, masked_score)
    sink_column = sink_logit.reshape(key_heads, group_size)[:, :, None]
    row_max = jnp.maximum(jnp.max(scores, axis=-1), sink_column)
    row_total = jnp.sum(jnp.exp(scores - row_max[..., None]), axis=-1) + jnp.exp(
        sink_column - row_max
    )
    log_total = row_max + jnp.log(row_total)
    soft_weights = jnp.exp(scores - log_total[..., None])
    soft_rounded = soft_weights.astype(jnp.bfloat16)
    attended = jnp.einsum(
        "kgqs,skd->qkgd", soft_rounded, band_values, preferred_element_type=jnp.float32
    ).astype(jnp.bfloat16)
    row_dots = jnp.sum(
        grad_heads.astype(jnp.float32) * attended.astype(jnp.float32), axis=-1
    ).transpose(1, 2, 0)
    prob_grads = jnp.einsum(
        "qkgd,skd->kgqs", grad_heads, band_values, preferred_element_type=jnp.float32
    )
    score_grads = (soft_weights * (prob_grads - row_dots[..., None])).astype(jnp.bfloat16)
    query_grads = (
        jnp.einsum("kgqs,skd->qkgd", score_grads, band_keys, preferred_element_type=jnp.float32)
        * scaling
    )
    query_grads = query_grads.astype(jnp.bfloat16).reshape(tok_rows, query_cols)
    band_key_grads = (
        jnp.einsum("kgqs,qkgd->skd", score_grads, query_heads, preferred_element_type=jnp.float32)
        * scaling
    )
    band_value_grads = jnp.einsum(
        "kgqs,qkgd->skd", soft_rounded, grad_heads, preferred_element_type=jnp.float32
    )
    band_grads = jnp.concatenate(
        [
            band_key_grads.reshape(band_rows, key_cols),
            band_value_grads.reshape(band_rows, key_cols),
        ],
        axis=1,
    )
    sink_part = -jnp.sum(jnp.exp(sink_column - log_total) * row_dots, axis=-1).reshape(-1)
    sink_grad = lax.psum(sink_part, "sp")
    attended_rows = attended.reshape(tok_rows, query_cols)
    input_block = lax.all_to_all(whole_input, "sp", 1, 0, tiled=True)
    grad_block = lax.all_to_all(whole_grad, "sp", 1, 0, tiled=True)
    early_rows = lax.all_gather(
        jnp.concatenate([query_grads, attended_rows], axis=1), "sp", axis=0, tiled=True
    )
    query_part = contract_rows(input_block, early_rows[:, :query_cols])
    out_part = contract_rows(early_rows[:, query_cols:], grad_block)
    returned_low = passed_along(band_grads[:WINDOW].astype(jnp.bfloat16), "sp", -1).astype(
        jnp.float32
    )
    returned_high = passed_along(
        band_grads[band_rows - WINDOW :].astype(jnp.bfloat16), "sp", 1
    ).astype(jnp.float32)
    own_rows = band_grads[WINDOW : WINDOW + tok_rows]
    own_rows = own_rows.at[tok_rows - WINDOW :].add(returned_low)
    own_rows = own_rows.at[:WINDOW].add(returned_high)
    key_grads = own_rows[:, :key_cols].astype(jnp.bfloat16)
    value_grads = own_rows[:, key_cols:].astype(jnp.bfloat16)
    late_rows = lax.all_gather(
        jnp.concatenate([key_grads, value_grads], axis=1), "sp", axis=0, tiled=True
    )
    key_part = contract_rows(input_block, late_rows[:, :key_cols])
    value_part = contract_rows(input_block, late_rows[:, key_cols:])
    partials = (
        contract_cols(query_grads, query_weight)
        + contract_cols(key_grads, key_weight)
        + contract_cols(value_grads, value_weight)
    )
    input_grad = lax.psum_scatter(
        partials.astype(jnp.bfloat16), "tp", scatter_dimension=1, tiled=True
    )
    return (input_grad, query_part, key_part, value_part, out_part, sink_grad)


LANES = 128
MESH = pl.DeviceIdType.MESH
VMEM_BYTES = 60 * 1024 * 1024


def dot_nn(a, b):
    return jnp.dot(a, b, preferred_element_type=jnp.float32)


def layer_kernel(
    x_ref, g_ref, wq_hbm, wk_hbm, wv_hbm, wo_hbm, sink_ref,
    ig_ref, gq_ref, gk_ref, gv_ref, go_ref, sg_ref,
    wq, wk, wv, wo, xg, acc, kvs, acts, att, dqs, dkv, cols,
    soft, sink_soft, sinks, part, rs_in,
    w_sem, ag_send, ag_recv, col_send, col_recv, y_send, y_recv, chip_send, chip_recv,
    z_sem, cross_sem, acts_recv, rs_send, rs_recv,
):
    bf16, f32 = jnp.bfloat16, jnp.float32
    count, tps = lax.axis_size("sp"), lax.axis_size("tp")
    depth = count // 2
    s, t = lax.axis_index("sp"), lax.axis_index("tp")
    z, x = s // 2, s % 2
    y, core = t // 2, t % 2
    partner = y * 2 + (1 - core)
    across = (1 - y) * 2 + core
    diag = (1 - y) * 2 + (1 - core)
    rows, feats = x_ref.shape
    q_cols, k_cols = wq.shape[1], wk.shape[1]
    block_cols = gq_ref.shape[0]
    per_slot = feats // block_cols
    key_heads = k_cols // HEAD
    group = q_cols // k_cols
    scaling = HEAD**-0.5

    def remote(src, dst, send, recv, dev_s, dev_t):
        return pltpu.make_async_remote_copy(
            src_ref=src, dst_ref=dst, send_sem=send, recv_sem=recv,
            device_id=(dev_s, dev_t), device_id_type=MESH,
        )

    weights = [
        pltpu.make_async_copy(src, dst, w_sem.at[i])
        for i, (src, dst) in enumerate(((wq_hbm, wq), (wk_hbm, wk), (wv_hbm, wv), (wo_hbm, wo)))
    ]
    for copy in weights:
        copy.start()

    barrier = pltpu.get_barrier_semaphore()
    for peer in (partner, across, diag):
        pl.semaphore_signal(barrier, inc=1, device_id=(s, peer), device_id_type=MESH)
    for d in range(1, count):
        pl.semaphore_signal(
            barrier, inc=1, device_id=((s + d) % count, t), device_id_type=MESH
        )
    pl.semaphore_wait(barrier, 3 + count - 1)

    sources = (x_ref, g_ref)
    to_across = [
        remote(sources[a], xg.at[t, a], ag_send.at[0, a], ag_recv.at[0, a], s, across)
        for a in range(2)
    ]
    to_partner = [
        remote(sources[a], xg.at[t, a], ag_send.at[1, a], ag_recv.at[1, a], s, partner)
        for a in range(2)
    ]
    relay = [
        remote(xg.at[across, a], xg.at[across, a], ag_send.at[2, a], ag_recv.at[2, a], s, partner)
        for a in range(2)
    ]
    for copy in to_across + to_partner:
        copy.start()

    is_home = s // per_slot == t
    is_across = s // per_slot == across
    is_last = jnp.logical_not(is_home | is_across)

    turn = [(s + d) % count for d in range(count)]

    def column_copy(a, b):
        span = pl.ds(b * block_cols, block_cols)
        source, slot = (g_ref.at[:, span], t) if a else (xg.at[across, 0, :, span], across)
        return remote(
            source, cols.at[a, s], col_send.at[a, b], col_recv.at[a, s], slot * per_slot + b, t
        )

    def column_arrival(a, source):
        ref = cols.at[a, source]
        return remote(ref, ref, col_send.at[a, 0], col_recv.at[a, source], turn[1], t)

    def y_copy(a, source):
        ref = cols.at[a, source]
        return remote(ref, ref, y_send.at[a, source], y_recv.at[a, source], s, across)

    def chip_copy(a, source):
        ref = cols.at[a, source]
        return remote(ref, ref, chip_send.at[a, source], chip_recv.at[a, source], s, partner)

    def each_column(a, act):
        slot = t if a else across
        for b in range(per_slot):

            @pl.when(slot * per_slot + b != s)
            def _():
                act(column_copy(a, b))

    def send_columns(a):
        each_column(a, lambda copy: copy.start())

    send_columns(1)

    def project_input(slot, first=False):
        cells = x_ref[...] if first else xg[slot, 0]
        span = pl.ds(pl.multiple_of(slot * feats, feats), feats)
        at = 0
        for w in (wq, wk, wv):
            wide = w.shape[1]
            term = dot_nn(cells, w[span, :])
            acc[:, at : at + wide] = term if first else acc[:, at : at + wide] + term
            at += wide

    def project_grad(slot, first=False):
        cells = g_ref[...] if first else xg[slot, 1]
        span = pl.ds(pl.multiple_of(slot * feats, feats), feats)
        term = contract_cols(cells, wo[:, span])
        lo = q_cols + 2 * k_cols
        acc[:, lo:] = term if first else acc[:, lo:] + term

    for edge in (0, WINDOW + count * rows):
        kvs[edge : edge + WINDOW] = jnp.zeros((WINDOW, 2 * k_cols), bf16)
    dkv[...] = jnp.zeros_like(dkv)
    sinks[...] = jnp.zeros_like(sinks)

    for copy in weights:
        copy.wait()
    project_input(t, True)
    project_grad(t, True)
    to_partner[0].wait_recv()
    project_input(partner)
    to_partner[1].wait_recv()
    project_grad(partner)
    to_across[0].wait_recv()
    relay[0].start()
    send_columns(0)
    project_input(across)
    relay[0].wait_recv()
    project_input(diag)
    for b in range(per_slot):
        span = slice(b * block_cols, (b + 1) * block_cols)

        @pl.when(t * per_slot + b == s)
        def _():
            cols[1, s] = g_ref[:, span]

        @pl.when(across * per_slot + b == s)
        def _():
            cols[0, s] = xg[across, 0, :, span]

    band_rows = rows + 2 * WINDOW
    tall = group * rows
    side_first = 1 - x

    def own_rows(block):
        return pl.ds(pl.multiple_of(WINDOW + block * rows, 32), rows)

    def band_at(block):
        return pl.ds(pl.multiple_of(block * rows, 32), band_rows)

    def item(i, block):
        return acts.at[i - 1, block] if i else kvs.at[own_rows(block)]

    def z_copy(i, block, way):
        dev = (z + 1 - 2 * way + depth) % depth * 2 + x
        ref = item(i, block)
        return remote(ref, ref, z_sem.at[way, i, block], acts_recv.at[i, block], dev, t)

    def cross_copy(i, block):
        ref = item(i, block)
        return remote(
            ref, ref, cross_sem.at[i, block], acts_recv.at[i, block], z * 2 + (1 - x), t
        )

    def goes_on(way):
        return jnp.where(way == 0, z < depth - 1, z > 0)

    def send_own(i):
        cross_copy(i, s).start()
        for way in range(2):

            @pl.when(goes_on(way))
            def _():
                z_copy(i, s, way).start()

    def level_at(d, way):
        level = z - d * (1 - 2 * way)
        return level, (level >= 0) & (level < depth)

    def forward(i, d):
        def one(k, _):
            way = lax.rem(side_first + k, 2)
            level, there = level_at(d, way)

            @pl.when(there)
            def _():
                block = level * 2 + x
                z_copy(i, block, way).wait_recv()
                cross_copy(i, block).start()

                @pl.when(goes_on(way))
                def _():
                    z_copy(i, block, way).start()

            return 0

        lax.fori_loop(0, 2, one, 0)

    kvs[own_rows(s)] = acc[:, q_cols : q_cols + 2 * k_cols].astype(bf16)
    send_own(0)
    acts[0, s] = acc[:, :q_cols].astype(bf16)
    send_own(1)

    to_across[1].wait_recv()
    relay[1].start()
    project_grad(across)
    relay[1].wait_recv()
    project_grad(diag)
    acts[1, s] = acc[:, q_cols + 2 * k_cols :].astype(bf16)
    send_own(2)

    def pass_direct(here, a):
        @pl.when(here)
        def _():
            for d, source in enumerate(turn):
                if d:
                    column_arrival(a, source).wait_recv()
                y_copy(a, source).start()
                chip_copy(a, source).start()

    def pass_second(here, a):
        @pl.when(here)
        def _():
            for source in turn:
                y_copy(a, source).wait_recv()
                chip_copy(a, source).start()

    def soften(block):
        row_at = lax.broadcasted_iota(jnp.int32, (tall, 1), 0)
        head_at = row_at // rows
        q_at = lax.broadcasted_iota(jnp.int32, (tall, band_rows), 0) - head_at * rows
        k_at = lax.broadcasted_iota(jnp.int32, (tall, band_rows), 1) - WINDOW
        k_pos = k_at + block * rows
        in_window = (
            (jnp.abs(q_at - k_at) <= WINDOW) & (k_pos >= 0) & (k_pos < rows * count)
        )
        for kh in range(key_heads):
            keys = kvs[band_at(block), kh * HEAD : (kh + 1) * HEAD]
            values = kvs[band_at(block), k_cols + kh * HEAD : k_cols + (kh + 1) * HEAD]
            heads = [kh * group + g for g in range(group)]
            q = jnp.concatenate(
                [acts[0, block, :, h * HEAD : (h + 1) * HEAD] for h in heads], axis=0
            )
            scores = jnp.where(in_window, contract_cols(q, keys) * scaling, masked_score)
            sink = jnp.full((tall, 1), sink_ref[0, kh * group], f32)
            for g in range(1, group):
                sink = jnp.where(head_at == g, sink_ref[0, kh * group + g], sink)
            top = jnp.maximum(jnp.max(scores, axis=1, keepdims=True), sink)
            e = jnp.exp(scores - top)
            sink_e = jnp.exp(sink - top)
            inverse = 1.0 / (jnp.sum(e, axis=1, keepdims=True) + sink_e)
            p = e * inverse
            soft[kh] = p
            sink_soft[kh] = jnp.broadcast_to(sink_e * inverse, (tall, LANES))
            attended = dot_nn(p.astype(bf16), values).astype(bf16)
            for g, h in enumerate(heads):
                att[block, :, h * HEAD : (h + 1) * HEAD] = attended[g * rows : (g + 1) * rows]

    def differentiate(block):
        lane_at = lax.broadcasted_iota(jnp.int32, (8, LANES), 1)
        sink_row = jnp.zeros((8, LANES), f32)
        for kh in range(key_heads):
            k_at = slice(kh * HEAD, (kh + 1) * HEAD)
            v_at = slice(k_cols + kh * HEAD, k_cols + (kh + 1) * HEAD)
            keys, values = kvs[band_at(block), k_at], kvs[band_at(block), v_at]
            heads = [kh * group + g for g in range(group)]
            q, do = (
                jnp.concatenate(
                    [acts[i, block, :, h * HEAD : (h + 1) * HEAD] for h in heads], axis=0
                )
                for i in range(2)
            )
            attended = jnp.concatenate(
                [att[block, :, h * HEAD : (h + 1) * HEAD] for h in heads], axis=0
            )
            dots = jnp.sum(do.astype(f32) * attended.astype(f32), axis=1, keepdims=True)
            p = soft[kh]
            ds = (p * (contract_cols(do, values) - dots)).astype(bf16)
            dq = (dot_nn(ds, keys) * scaling).astype(bf16)
            sink_terms = sink_soft[kh] * dots
            for g, h in enumerate(heads):
                dqs[block, :, h * HEAD : (h + 1) * HEAD] = dq[g * rows : (g + 1) * rows]
                total = -jnp.sum(sink_terms[g * rows : (g + 1) * rows], axis=0, keepdims=True)
                sink_row = jnp.where(lane_at == h, total, sink_row)
            dkv[band_at(block), k_at] += contract_rows(ds, q)
            dkv[band_at(block), v_at] += contract_rows(p.astype(bf16), do)
        sinks[...] += sink_row

    def cross_arrived(i, level):
        cross_copy(i, level * 2 + (1 - x)).wait_recv()

    def attend_own():
        for i in range(3):
            cross_arrived(i, z)

        @pl.when((z == 0) | (z == depth - 1))
        def _():
            block = jnp.where(z == 0, 0, count - 1)
            soften(block)
            differentiate(block)

    def attend(d, way, begin=0, end=None):
        level, there = level_at(d, way)
        cross = level * 2 + (1 - x)
        extra = jnp.where(jnp.where(way == 0, level == 0, level == depth - 1), 1, 0)
        stop = 2 + extra
        nearest = jnp.where(way == 0, 2 * level + 2, 2 * level - 1)
        step = jnp.where(way == 0, -1, 1)
        inside = (x == way) | (extra == 1)
        key_at = jnp.where(x == way, 0, 1)

        def one(k, _):
            is_end = k == stop - 1
            block = nearest + step * k
            passed = jnp.where(way == 0, block <= cross, block >= cross)
            block = jnp.where(inside & passed, block + step, block)
            block = jnp.where(inside & is_end, cross, block)

            @pl.when(k == key_at)
            def _():
                cross_arrived(0, level)

            @pl.when(is_end)
            def _():
                cross_arrived(1, level)

            soften(block)

            @pl.when(is_end)
            def _():
                cross_arrived(2, level)

            differentiate(block)
            return 0

        last = stop if end is None else jnp.minimum(stop, end)
        lax.fori_loop(begin, jnp.where(there, last, begin), one, 0)

    def attend_both(d):
        lax.fori_loop(0, 2, lambda k, _: attend(d, lax.rem(x + k, 2)) or 0, 0)

    def attended_range(d):
        first = jnp.where(z <= d, 0, 2 * (z - d) + 1)
        last = jnp.where(z + d >= depth - 1, count - 1, 2 * (z + d))
        return first, last + 1

    def consume(block, first=False):
        pieces = (
            (go_ref, contract_rows(att[block], cols[1, block])),
            (gq_ref, contract_rows(cols[0, block], dqs[block])),
        )
        for ref, value in pieces:
            ref[...] += value

    def consume_range(begin, end):
        lax.fori_loop(begin, end, lambda block, _: consume(block) or 0, 0)

    def consume_since(d):
        before, now = attended_range(d - 1), attended_range(d)
        consume_range(now[0], before[0])
        consume_range(before[1], now[1])

    pass_direct(is_home, 1)
    forward(0, 1)
    forward(1, 1)
    attend_own()
    forward(2, 1)
    pass_direct(is_across, 0)
    forward(0, 2)
    forward(1, 2)
    attend(1, x)
    attend(1, 1 - x, 0, 1)
    forward(2, 2)
    pass_second(is_across, 1)
    own_dkv = dkv[own_rows(s)]
    own_dk = (own_dkv[:, :k_cols] * scaling).astype(bf16)
    own_dv = own_dkv[:, k_cols:].astype(bf16)

    def partial_for(slot):
        span = pl.ds(pl.multiple_of(slot * feats, feats), feats)
        return (
            contract_cols(dqs[s], wq[span, :])
            + contract_cols(own_dk, wk[span, :])
            + contract_cols(own_dv, wv[span, :])
        )

    rs_copies = [
        remote(part.at[i], rs_in.at[i], rs_send.at[i], rs_recv.at[i], s, peer)
        for i, peer in enumerate((partner, partner, across))
    ]
    for i, slot in enumerate((diag, partner)):
        part[i] = partial_for(slot).astype(bf16)
        rs_copies[i].start()
    far = partial_for(across)
    rs_copies[0].wait_recv()
    part[2] = (far + rs_in[0].astype(f32)).astype(bf16)
    rs_copies[2].start()
    ig_acc = acc.at[:, :feats]
    ig_acc[...] = partial_for(t)
    go_ref[...] = jnp.zeros_like(go_ref)
    gq_ref[...] = jnp.zeros_like(gq_ref)

    for d in range(3, depth):
        forward(0, d)
        forward(1, d)
    attend(1, 1 - x, 1)
    pass_second(is_home, 0)
    @pl.when(is_last)
    def _():
        for source in range(count):
            for a in range(2):
                chip_copy(a, source).wait_recv()

    consume_range(*attended_range(1))
    attend_both(2)
    for d in range(3, depth):
        forward(2, d)
    consume_since(2)
    for copy in rs_copies[1:]:
        copy.wait_recv()
    ig_ref[...] = (
        ig_acc[...] + rs_in[1].astype(f32) + rs_in[2].astype(f32)
    ).astype(bf16)
    for d in range(3, depth):
        attend_both(d)
        consume_since(d)
    sg_ref[...] = sinks[...]
    seq = pl.ds(WINDOW, count * rows)
    left = cols[0].reshape(count * rows, block_cols)
    gk_ref[...] = contract_rows(left, (dkv[seq, :k_cols] * scaling).astype(bf16))
    gv_ref[...] = contract_rows(left, dkv[seq, k_cols:].astype(bf16))

    for copy in to_across + to_partner + relay + rs_copies:
        copy.wait_send()
    for a in range(2):
        each_column(a, lambda copy: copy.wait_send())
        for source in range(count):

            @pl.when(is_home if a else is_across)
            def _():
                y_copy(a, source).wait_send()

            @pl.when(jnp.logical_not(is_last))
            def _():
                chip_copy(a, source).wait_send()

    for i in range(3):
        for level in range(depth):
            block = level * 2 + x
            for way in range(2):
                came = jnp.where(way == 0, level <= z, level >= z)

                @pl.when(came & goes_on(way))
                def _():
                    z_copy(i, block, way).wait_send()

            cross_copy(i, block).wait_send()


def store_kernel(*refs):
    ins, sink_in, outs, sink_out = refs[:5], refs[5], refs[6:11], refs[11]
    held, in_sem, out_sem = refs[12:17], refs[17], refs[18]
    loads = [pltpu.make_async_copy(ins[i], held[i], in_sem.at[i]) for i in range(5)]
    stores = [pltpu.make_async_copy(held[i], outs[i], out_sem.at[i]) for i in range(5)]
    for load in loads:
        load.start()
    sink_out[...] = sink_in[0:1, : sink_out.shape[1]]
    for load, store in zip(loads, stores):
        load.wait()
        store.start()
    for store in stores:
        store.wait()


def fused_device(
    layer_input, output_grad, query_weight, key_weight, value_weight, out_weight, sink_logit
):
    bf16, f32 = jnp.bfloat16, jnp.float32
    count, tps = lax.axis_size("sp"), lax.axis_size("tp")
    rows, feats = layer_input.shape
    width = query_weight.shape[0]
    q_cols, k_cols = query_weight.shape[1], key_weight.shape[1]
    block_cols = width // count
    vmem = pl.BlockSpec(memory_space=pltpu.VMEM)
    hbm = pl.BlockSpec(memory_space=pl.ANY)
    dma = pltpu.SemaphoreType.DMA
    outs = pl.pallas_call(
        layer_kernel,
        out_shape=(
            jax.ShapeDtypeStruct((rows, feats), bf16),
            jax.ShapeDtypeStruct((block_cols, q_cols), f32),
            jax.ShapeDtypeStruct((block_cols, k_cols), f32),
            jax.ShapeDtypeStruct((block_cols, k_cols), f32),
            jax.ShapeDtypeStruct((q_cols, block_cols), f32),
            jax.ShapeDtypeStruct((8, LANES), f32),
        ),
        in_specs=[vmem, vmem, hbm, hbm, hbm, hbm, pl.BlockSpec(memory_space=pltpu.SMEM)],
        out_specs=(vmem,) * 6,
        scratch_shapes=[
            pltpu.VMEM(query_weight.shape, bf16),
            pltpu.VMEM(key_weight.shape, bf16),
            pltpu.VMEM(value_weight.shape, bf16),
            pltpu.VMEM(out_weight.shape, bf16),
            pltpu.VMEM((tps, 2, rows, feats), bf16),
            pltpu.VMEM((rows, 2 * q_cols + 2 * k_cols), f32),
            pltpu.VMEM((count * rows + 2 * WINDOW, 2 * k_cols), bf16),
            pltpu.VMEM((2, count, rows, q_cols), bf16),
            pltpu.VMEM((count, rows, q_cols), bf16),
            pltpu.VMEM((count, rows, q_cols), bf16),
            pltpu.VMEM((count * rows + 2 * WINDOW, 2 * k_cols), f32),
            pltpu.VMEM((2, count, rows, block_cols), bf16),
            pltpu.VMEM((k_cols // HEAD, q_cols // k_cols * rows, rows + 2 * WINDOW), f32),
            pltpu.VMEM((k_cols // HEAD, q_cols // k_cols * rows, LANES), f32),
            pltpu.VMEM((8, LANES), f32),
            pltpu.VMEM((3, rows, feats), bf16),
            pltpu.VMEM((3, rows, feats), bf16),
            dma((4,)), dma((3, 2)), dma((3, 2)),
            dma((2, feats // block_cols)), dma((2, count)),
            dma((2, count)), dma((2, count)), dma((2, count)), dma((2, count)),
            dma((2, 3, count)), dma((3, count)), dma((3, count)), dma((3,)), dma((3,)),
        ],
        compiler_params=pltpu.CompilerParams(
            collective_id=0, has_side_effects=True, vmem_limit_bytes=VMEM_BYTES
        ),
        name="layer",
    )(
        layer_input, output_grad, query_weight, key_weight, value_weight, out_weight,
        sink_logit.reshape(1, -1),
    )
    kept = [jax.ShapeDtypeStruct(out.shape, out.dtype) for out in outs[:5]]
    stored = pl.pallas_call(
        store_kernel,
        out_shape=(*kept, jax.ShapeDtypeStruct((1, sink_logit.shape[0]), f32)),
        in_specs=[hbm] * 5 + [vmem],
        out_specs=(hbm,) * 5 + (vmem,),
        scratch_shapes=[pltpu.VMEM(out.shape, out.dtype) for out in kept]
        + [dma((5,)), dma((5,))],
        compiler_params=pltpu.CompilerParams(vmem_limit_bytes=VMEM_BYTES),
        name="store",
    )(*outs)
    return tuple(stored[:5]) + (stored[5].reshape(-1),)


def fits_kernel(mesh, layer_width):
    count, tps = mesh.shape["sp"], mesh.shape["tp"]
    return tps == 4 and count % 8 == 0 and layer_width == count * tps * LANES and HEADS == 2 * KV_HEADS


def solution(mesh):
    placed = (
        P("sp", "tp"),
        P("sp", "tp"),
        P(None, "tp"),
        P(None, "tp"),
        P(None, "tp"),
        P("tp", None),
        P("tp"),
    )

    def sharded(*arrays):
        width = arrays[0].shape[1]
        body = fused_device if fits_kernel(mesh, width) else per_device
        return jax.shard_map(
            body,
            mesh=mesh,
            in_specs=placed,
            out_specs=(
                P("sp", "tp"),
                P("sp", "tp"),
                P("sp", "tp"),
                P("sp", "tp"),
                P("tp", "sp"),
                P("tp"),
            ),
            check_vma=False,
        )(*arrays)

    return sharded
```

time: 89.9 us -> 86.2 us (0.959)
  Pallas kernels: 87.5 us -> 84.3 us
    pallas_call x1, Pallas kernels: 83.2 us -> 80 us  [fused_device(): pl.pallas_call(layer_kernel, out_shape=(jax.ShapeDtypeStruct((rows, feats...]
where the time goes in v1:
time: 86.2 us; the launch traced here: 85.1 us
  Pallas kernels  84.3 us (98%)
    pallas_call x1, Pallas kernels, fused_device(): pl.pallas_call(layer_kernel, out_shape=(jax.ShapeDtypeStruct((rows, feats...  80 us
    pallas_call x1, Pallas kernels, fused_device(): pl.pallas_call(store_kernel, out_shape=(*kept, jax.ShapeDtypeStruct((1, s...  4.33 us

profile of v1, /device:TPU:0, one launch (start us, length us, event | category | flops | bytes accessed | tf_op | source)
XLA Modules:
  0.0 85.1 jit_solution(10046900896197855099)
XLA Ops:
  0.6 80.0 %layer.1 = (bf16[160,1024]{1,0:T(8,128)(2,1)}, f32[512,512]{1,0:T(8,128)}, f32[512,256]{1,0:T(8,128)}, f32[512,256]{1,0:T(8,128)}, f32[512,512]{1,0:T(8,128)}, /*index=5*/f32[8,128]{1,0:T(8,128)}) custom-call(bf16[160,1024]{1,0:T(8,128)(2,1)} %x_ref.1, bf16[160,1024]{1,0:T(8,128)(2,1)} %g_ref.1, bf16[4096,512]{1,0:T(8,128)(2,1)} %wq_hbm.1, ...), custom_call_target="tpu_custom_call" | custom-call | tf_op jit(solution)/shard_map/layer/pallas_call | solution.py:675
  80.6 4.3 %store.1 = (bf16[160,1024]{1,0:T(8,128)(2,1)}, f32[512,512]{1,0:T(8,128)}, f32[512,256]{1,0:T(8,128)}, f32[512,256]{1,0:T(8,128)}, f32[512,512]{1,0:T(8,128)}, /*index=5*/f32[1,4]{1,0:T(1,128)}) custom-call(bf16[160,1024]{1,0:T(8,128)(2,1)} %get-tuple-element.18.refs_0_, f32[512,512]{1,0:T(8,128)} %get-tuple-element.19.refs_1_, ...), custom_call_target="tpu_custom_call" | custom-call | tf_op jit(solution)/shard_map/store/pallas_call | solution.py:719

commit v2 on v1

--- a/solution.py
+++ b/solution.py
@@ -170,8 +170,10 @@
 
 
 LANES = 128
+LOG2E = 1.4426950408889634
 MESH = pl.DeviceIdType.MESH
-VMEM_BYTES = 60 * 1024 * 1024
+VMEM_BYTES = 46 * 1024 * 1024
+STORE_BYTES = 8 * 1024 * 1024
 
 
 def dot_nn(a, b):
@@ -179,10 +181,9 @@
 
 
 def layer_kernel(
-    x_ref, g_ref, wq_hbm, wk_hbm, wv_hbm, wo_hbm, sink_ref,
+    x_hbm, g_hbm, wq_hbm, wk_hbm, wv_hbm, wo_hbm, sink_hbm,
     ig_ref, gq_ref, gk_ref, gv_ref, go_ref, sg_ref,
-    wq, wk, wv, wo, xg, acc, kvs, acts, att, dqs, dkv, cols,
-    soft, sink_soft, sinks, part, rs_in,
+    w_in, wo, xg, acc, kvs, acts, att, dqs, dkv, cols, bias, sinks, part, rs_in, sink_ref,
     w_sem, ag_send, ag_recv, col_send, col_recv, y_send, y_recv, chip_send, chip_recv,
     z_sem, cross_sem, acts_recv, rs_send, rs_recv,
 ):
@@ -195,8 +196,9 @@
     partner = y * 2 + (1 - core)
     across = (1 - y) * 2 + core
     diag = (1 - y) * 2 + (1 - core)
-    rows, feats = x_ref.shape
-    q_cols, k_cols = wq.shape[1], wk.shape[1]
+    rows, feats = x_hbm.shape
+    q_cols, k_cols = wq_hbm.shape[1], wk_hbm.shape[1]
+    in_cols = q_cols + 2 * k_cols
     block_cols = gq_ref.shape[0]
     per_slot = feats // block_cols
     key_heads = k_cols // HEAD
@@ -209,10 +211,19 @@
             device_id=(dev_s, dev_t), device_id_type=MESH,
         )
 
-    weights = [
-        pltpu.make_async_copy(src, dst, w_sem.at[i])
-        for i, (src, dst) in enumerate(((wq_hbm, wq), (wk_hbm, wk), (wv_hbm, wv), (wo_hbm, wo)))
+    own = [
+        pltpu.make_async_copy(src, xg.at[t, a], w_sem.at[4 + a])
+        for a, src in enumerate((x_hbm, g_hbm))
     ]
+    for copy in own:
+        copy.start()
+    weights, at = [], 0
+    for i, src in enumerate((wq_hbm, wk_hbm, wv_hbm)):
+        span = pl.ds(at, src.shape[1])
+        weights.append(pltpu.make_async_copy(src, w_in.at[:, span], w_sem.at[i]))
+        at += src.shape[1]
+    weights.append(pltpu.make_async_copy(wo_hbm, wo, w_sem.at[3]))
+    weights.append(pltpu.make_async_copy(sink_hbm, sink_ref, w_sem.at[6]))
     for copy in weights:
         copy.start()
 
@@ -225,7 +236,9 @@
         )
     pl.semaphore_wait(barrier, 3 + count - 1)
 
-    sources = (x_ref, g_ref)
+    sources = (xg.at[t, 0], xg.at[t, 1])
+    for copy in own:
+        copy.wait()
     to_across = [
         remote(sources[a], xg.at[t, a], ag_send.at[0, a], ag_recv.at[0, a], s, across)
         for a in range(2)
@@ -249,7 +262,7 @@
 
     def column_copy(a, b):
         span = pl.ds(b * block_cols, block_cols)
-        source, slot = (g_ref.at[:, span], t) if a else (xg.at[across, 0, :, span], across)
+        source, slot = (xg.at[t, 1, :, span], t) if a else (xg.at[across, 0, :, span], across)
         return remote(
             source, cols.at[a, s], col_send.at[a, b], col_recv.at[a, s], slot * per_slot + b, t
         )
@@ -280,26 +293,34 @@
     send_columns(1)
 
     def project_input(slot, first=False):
-        cells = x_ref[...] if first else xg[slot, 0]
+        cells = xg[slot, 0]
         span = pl.ds(pl.multiple_of(slot * feats, feats), feats)
-        at = 0
-        for w in (wq, wk, wv):
-            wide = w.shape[1]
-            term = dot_nn(cells, w[span, :])
-            acc[:, at : at + wide] = term if first else acc[:, at : at + wide] + term
-            at += wide
+        term = dot_nn(cells, w_in[span, :])
+        acc[:, :in_cols] = term if first else acc[:, :in_cols] + term
 
     def project_grad(slot, first=False):
-        cells = g_ref[...] if first else xg[slot, 1]
+        cells = xg[slot, 1]
         span = pl.ds(pl.multiple_of(slot * feats, feats), feats)
         term = contract_cols(cells, wo[:, span])
-        lo = q_cols + 2 * k_cols
-        acc[:, lo:] = term if first else acc[:, lo:] + term
+        acc[:, in_cols:] = term if first else acc[:, in_cols:] + term
 
     for edge in (0, WINDOW + count * rows):
         kvs[edge : edge + WINDOW] = jnp.zeros((WINDOW, 2 * k_cols), bf16)
     dkv[...] = jnp.zeros_like(dkv)
     sinks[...] = jnp.zeros_like(sinks)
+    part_rows = rows // 2
+    part_keys = part_rows + 2 * WINDOW
+    tall = group * part_rows
+    edges = -(-WINDOW // part_rows)
+    parts = rows * count // part_rows
+    q_at = lax.rem(lax.broadcasted_iota(jnp.int32, (tall, part_keys), 0), part_rows)
+    k_at = lax.broadcasted_iota(jnp.int32, (tall, part_keys), 1)
+    band = (k_at >= q_at) & (k_at - q_at <= 2 * WINDOW)
+    starts = [edges] + list(range(edges)) + [parts - edges + i for i in range(edges)]
+    for i, start in enumerate(starts):
+        pos = k_at + (start * part_rows - WINDOW)
+        inside = band & (pos >= 0) & (pos < rows * count) if i else band
+        bias[i] = jnp.where(inside, 0.0, masked_score)
 
     for copy in weights:
         copy.wait()
@@ -320,21 +341,16 @@
 
         @pl.when(t * per_slot + b == s)
         def _():
-            cols[1, s] = g_ref[:, span]
+            cols[1, s] = xg[t, 1, :, span]
 
         @pl.when(across * per_slot + b == s)
         def _():
             cols[0, s] = xg[across, 0, :, span]
 
-    band_rows = rows + 2 * WINDOW
-    tall = group * rows
     side_first = 1 - x
 
     def own_rows(block):
         return pl.ds(pl.multiple_of(WINDOW + block * rows, 32), rows)
-
-    def band_at(block):
-        return pl.ds(pl.multiple_of(block * rows, 32), band_rows)
 
     def item(i, block):
         return acts.at[i - 1, block] if i else kvs.at[own_rows(block)]
@@ -384,7 +400,7 @@
 
         lax.fori_loop(0, 2, one, 0)
 
-    kvs[own_rows(s)] = acc[:, q_cols : q_cols + 2 * k_cols].astype(bf16)
+    kvs[own_rows(s)] = acc[:, q_cols:in_cols].astype(bf16)
     send_own(0)
     acts[0, s] = acc[:, :q_cols].astype(bf16)
     send_own(1)
@@ -394,7 +410,7 @@
     project_grad(across)
     relay[1].wait_recv()
     project_grad(diag)
-    acts[1, s] = acc[:, q_cols + 2 * k_cols :].astype(bf16)
+    acts[1, s] = acc[:, in_cols:].astype(bf16)
     send_own(2)
 
     def pass_direct(here, a):
@@ -413,66 +429,78 @@
                 y_copy(a, source).wait_recv()
                 chip_copy(a, source).start()
 
-    def soften(block):
-        row_at = lax.broadcasted_iota(jnp.int32, (tall, 1), 0)
-        head_at = row_at // rows
-        q_at = lax.broadcasted_iota(jnp.int32, (tall, band_rows), 0) - head_at * rows
-        k_at = lax.broadcasted_iota(jnp.int32, (tall, band_rows), 1) - WINDOW
-        k_pos = k_at + block * rows
-        in_window = (
-            (jnp.abs(q_at - k_at) <= WINDOW) & (k_pos >= 0) & (k_pos < rows * count)
-        )
-        for kh in range(key_heads):
-            keys = kvs[band_at(block), kh * HEAD : (kh + 1) * HEAD]
-            values = kvs[band_at(block), k_cols + kh * HEAD : k_cols + (kh + 1) * HEAD]
+    def attend_block(block):
+        jobs = [(half_at, kh) for half_at in range(2) for kh in range(key_heads)]
+        each = range(len(jobs))
+        head_at = lax.broadcasted_iota(jnp.int32, (tall, 1), 0) // part_rows
+
+        def at(half_at):
+            start = block * rows + half_at * part_rows
+            return pl.ds(pl.multiple_of(start, 16), part_keys)
+
+        def stacked(i, half_at, kh):
+            span = slice(half_at * part_rows, (half_at + 1) * part_rows)
             heads = [kh * group + g for g in range(group)]
-            q = jnp.concatenate(
-                [acts[0, block, :, h * HEAD : (h + 1) * HEAD] for h in heads], axis=0
+            return jnp.concatenate(
+                [acts[i, block, span, h * HEAD : (h + 1) * HEAD] for h in heads], axis=0
             )
-            scores = jnp.where(in_window, contract_cols(q, keys) * scaling, masked_score)
-            sink = jnp.full((tall, 1), sink_ref[0, kh * group], f32)
+
+        def k_lanes(kh):
+            return slice(kh * HEAD, (kh + 1) * HEAD)
+
+        def v_lanes(kh):
+            return slice(k_cols + kh * HEAD, k_cols + (kh + 1) * HEAD)
+
+        which = []
+        for half_at, _ in jobs:
+            part_at = block * 2 + half_at
+            late = part_at - (parts - edges)
+            which.append(
+                jnp.where(part_at < edges, 1 + part_at, jnp.where(late >= 0, 1 + edges + late, 0))
+            )
+        q = [stacked(0, *job) for job in jobs]
+        do = [stacked(1, *job) for job in jobs]
+        keys = [kvs[at(half_at), k_lanes(kh)] for half_at, kh in jobs]
+        values = [kvs[at(half_at), v_lanes(kh)] for half_at, kh in jobs]
+        scores = [contract_cols(q[i], keys[i]) for i in each]
+        prob_grads = [contract_cols(do[i], values[i]) for i in each]
+        scores = [scores[i] * (scaling * LOG2E) + bias[which[i]] for i in each]
+        sink = []
+        for _, kh in jobs:
+            column = jnp.full((tall, 1), sink_ref[0, kh * group], f32)
             for g in range(1, group):
-                sink = jnp.where(head_at == g, sink_ref[0, kh * group + g], sink)
-            top = jnp.maximum(jnp.max(scores, axis=1, keepdims=True), sink)
-            e = jnp.exp(scores - top)
-            sink_e = jnp.exp(sink - top)
-            inverse = 1.0 / (jnp.sum(e, axis=1, keepdims=True) + sink_e)
-            p = e * inverse
-            soft[kh] = p
-            sink_soft[kh] = jnp.broadcast_to(sink_e * inverse, (tall, LANES))
-            attended = dot_nn(p.astype(bf16), values).astype(bf16)
-            for g, h in enumerate(heads):
-                att[block, :, h * HEAD : (h + 1) * HEAD] = attended[g * rows : (g + 1) * rows]
-
-    def differentiate(block):
+                column = jnp.where(head_at == g, sink_ref[0, kh * group + g], column)
+            sink.append(column * LOG2E)
+        top = [jnp.maximum(jnp.max(scores[i], axis=1, keepdims=True), sink[i]) for i in each]
+        e = [jnp.exp2(scores[i] - top[i]) for i in each]
+        sink_e = [jnp.exp2(sink[i] - top[i]) for i in each]
+        inverse = [1.0 / (jnp.sum(e[i], axis=1, keepdims=True) + sink_e[i]) for i in each]
+        p = [e[i] * inverse[i] for i in each]
+        p_low = [p[i].astype(bf16) for i in each]
+        attended = [dot_nn(p_low[i], values[i]).astype(bf16) for i in each]
+        dots = [
+            jnp.sum(do[i].astype(f32) * attended[i].astype(f32), axis=1, keepdims=True)
+            for i in each
+        ]
+        dv = [contract_rows(p_low[i], do[i]) for i in each]
+        ds = [(p[i] * (prob_grads[i] - dots[i])).astype(bf16) for i in each]
+        dq = [(dot_nn(ds[i], keys[i]) * scaling).astype(bf16) for i in each]
+        dk = [contract_rows(ds[i], q[i]) for i in each]
         lane_at = lax.broadcasted_iota(jnp.int32, (8, LANES), 1)
-        sink_row = jnp.zeros((8, LANES), f32)
-        for kh in range(key_heads):
-            k_at = slice(kh * HEAD, (kh + 1) * HEAD)
-            v_at = slice(k_cols + kh * HEAD, k_cols + (kh + 1) * HEAD)
-            keys, values = kvs[band_at(block), k_at], kvs[band_at(block), v_at]
-            heads = [kh * group + g for g in range(group)]
-            q, do = (
-                jnp.concatenate(
-                    [acts[i, block, :, h * HEAD : (h + 1) * HEAD] for h in heads], axis=0
-                )
-                for i in range(2)
-            )
-            attended = jnp.concatenate(
-                [att[block, :, h * HEAD : (h + 1) * HEAD] for h in heads], axis=0
-            )
-            dots = jnp.sum(do.astype(f32) * attended.astype(f32), axis=1, keepdims=True)
-            p = soft[kh]
-            ds = (p * (contract_cols(do, values) - dots)).astype(bf16)
-            dq = (dot_nn(ds, keys) * scaling).astype(bf16)
-            sink_terms = sink_soft[kh] * dots
-            for g, h in enumerate(heads):
-                dqs[block, :, h * HEAD : (h + 1) * HEAD] = dq[g * rows : (g + 1) * rows]
-                total = -jnp.sum(sink_terms[g * rows : (g + 1) * rows], axis=0, keepdims=True)
-                sink_row = jnp.where(lane_at == h, total, sink_row)
-            dkv[band_at(block), k_at] += contract_rows(ds, q)
-            dkv[band_at(block), v_at] += contract_rows(p.astype(bf16), do)
-        sinks[...] += sink_row
+        sink_row = sinks[...]
+        for i, (half_at, kh) in enumerate(jobs):
+            span = slice(half_at * part_rows, (half_at + 1) * part_rows)
+            sink_terms = sink_e[i] * inverse[i] * dots[i]
+            for g in range(group):
+                h = kh * group + g
+                lanes, piece = slice(h * HEAD, (h + 1) * HEAD), slice(g * part_rows, (g + 1) * part_rows)
+                att[block, span, lanes] = attended[i][piece]
+                dqs[block, span, lanes] = dq[i][piece]
+                total = jnp.sum(sink_terms[piece], axis=0, keepdims=True)
+                sink_row = jnp.where(lane_at == h, sink_row - total, sink_row)
+            dkv[at(half_at), k_lanes(kh)] += dk[i]
+            dkv[at(half_at), v_lanes(kh)] += dv[i]
+        sinks[...] = sink_row
 
     def cross_arrived(i, level):
         cross_copy(i, level * 2 + (1 - x)).wait_recv()
@@ -484,8 +512,7 @@
         @pl.when((z == 0) | (z == depth - 1))
         def _():
             block = jnp.where(z == 0, 0, count - 1)
-            soften(block)
-            differentiate(block)
+            attend_block(block)
 
     def attend(d, way, begin=0, end=None):
         level, there = level_at(d, way)
@@ -511,14 +538,9 @@
             @pl.when(is_end)
             def _():
                 cross_arrived(1, level)
-
-            soften(block)
-
-            @pl.when(is_end)
-            def _():
                 cross_arrived(2, level)
 
-            differentiate(block)
+            attend_block(block)
             return 0
 
         last = stop if end is None else jnp.minimum(stop, end)
@@ -526,27 +548,6 @@
 
     def attend_both(d):
         lax.fori_loop(0, 2, lambda k, _: attend(d, lax.rem(x + k, 2)) or 0, 0)
-
-    def attended_range(d):
-        first = jnp.where(z <= d, 0, 2 * (z - d) + 1)
-        last = jnp.where(z + d >= depth - 1, count - 1, 2 * (z + d))
-        return first, last + 1
-
-    def consume(block, first=False):
-        pieces = (
-            (go_ref, contract_rows(att[block], cols[1, block])),
-            (gq_ref, contract_rows(cols[0, block], dqs[block])),
-        )
-        for ref, value in pieces:
-            ref[...] += value
-
-    def consume_range(begin, end):
-        lax.fori_loop(begin, end, lambda block, _: consume(block) or 0, 0)
-
-    def consume_since(d):
-        before, now = attended_range(d - 1), attended_range(d)
-        consume_range(now[0], before[0])
-        consume_range(before[1], now[1])
 
     pass_direct(is_home, 1)
     forward(0, 1)
@@ -561,16 +562,18 @@
     forward(2, 2)
     pass_second(is_across, 1)
     own_dkv = dkv[own_rows(s)]
-    own_dk = (own_dkv[:, :k_cols] * scaling).astype(bf16)
-    own_dv = own_dkv[:, k_cols:].astype(bf16)
+    own_grads = jnp.concatenate(
+        [
+            dqs[s],
+            (own_dkv[:, :k_cols] * scaling).astype(bf16),
+            own_dkv[:, k_cols:].astype(bf16),
+        ],
+        axis=1,
+    )
 
     def partial_for(slot):
         span = pl.ds(pl.multiple_of(slot * feats, feats), feats)
-        return (
-            contract_cols(dqs[s], wq[span, :])
-            + contract_cols(own_dk, wk[span, :])
-            + contract_cols(own_dv, wv[span, :])
-        )
+        return contract_cols(own_grads, w_in[span, :])
 
     rs_copies = [
         remote(part.at[i], rs_in.at[i], rs_send.at[i], rs_recv.at[i], s, peer)
@@ -585,8 +588,6 @@
     rs_copies[2].start()
     ig_acc = acc.at[:, :feats]
     ig_acc[...] = partial_for(t)
-    go_ref[...] = jnp.zeros_like(go_ref)
-    gq_ref[...] = jnp.zeros_like(gq_ref)
 
     for d in range(3, depth):
         forward(0, d)
@@ -599,11 +600,9 @@
             for a in range(2):
                 chip_copy(a, source).wait_recv()
 
-    consume_range(*attended_range(1))
     attend_both(2)
     for d in range(3, depth):
         forward(2, d)
-    consume_since(2)
     for copy in rs_copies[1:]:
         copy.wait_recv()
     ig_ref[...] = (
@@ -611,10 +610,13 @@
     ).astype(bf16)
     for d in range(3, depth):
         attend_both(d)
-        consume_since(d)
     sg_ref[...] = sinks[...]
     seq = pl.ds(WINDOW, count * rows)
     left = cols[0].reshape(count * rows, block_cols)
+    go_ref[...] = contract_rows(
+        att[...].reshape(count * rows, q_cols), cols[1].reshape(count * rows, block_cols)
+    )
+    gq_ref[...] = contract_rows(left, dqs[...].reshape(count * rows, q_cols))
     gk_ref[...] = contract_rows(left, (dkv[seq, :k_cols] * scaling).astype(bf16))
     gv_ref[...] = contract_rows(left, dkv[seq, k_cols:].astype(bf16))
 
@@ -646,16 +648,11 @@
 
 
 def store_kernel(*refs):
-    ins, sink_in, outs, sink_out = refs[:5], refs[5], refs[6:11], refs[11]
-    held, in_sem, out_sem = refs[12:17], refs[17], refs[18]
-    loads = [pltpu.make_async_copy(ins[i], held[i], in_sem.at[i]) for i in range(5)]
-    stores = [pltpu.make_async_copy(held[i], outs[i], out_sem.at[i]) for i in range(5)]
-    for load in loads:
-        load.start()
+    ins, sink_in, outs, sink_out, sem = refs[:5], refs[5], refs[6:11], refs[11], refs[12]
+    stores = [pltpu.make_async_copy(ins[i], outs[i], sem.at[i]) for i in range(5)]
+    for store in stores:
+        store.start()
     sink_out[...] = sink_in[0:1, : sink_out.shape[1]]
-    for load, store in zip(loads, stores):
-        load.wait()
-        store.start()
     for store in stores:
         store.wait()
 
@@ -670,7 +667,7 @@
     q_cols, k_cols = query_weight.shape[1], key_weight.shape[1]
     block_cols = width // count
     vmem = pl.BlockSpec(memory_space=pltpu.VMEM)
-    hbm = pl.BlockSpec(memory_space=pl.ANY)
+    hbm = pl.BlockSpec(memory_space=pltpu.HBM)
     dma = pltpu.SemaphoreType.DMA
     outs = pl.pallas_call(
         layer_kernel,
@@ -682,12 +679,10 @@
             jax.ShapeDtypeStruct((q_cols, block_cols), f32),
             jax.ShapeDtypeStruct((8, LANES), f32),
         ),
-        in_specs=[vmem, vmem, hbm, hbm, hbm, hbm, pl.BlockSpec(memory_space=pltpu.SMEM)],
+        in_specs=[hbm] * 7,
         out_specs=(vmem,) * 6,
         scratch_shapes=[
-            pltpu.VMEM(query_weight.shape, bf16),
-            pltpu.VMEM(key_weight.shape, bf16),
-            pltpu.VMEM(value_weight.shape, bf16),
+            pltpu.VMEM((width, q_cols + 2 * k_cols), bf16),
             pltpu.VMEM(out_weight.shape, bf16),
             pltpu.VMEM((tps, 2, rows, feats), bf16),
             pltpu.VMEM((rows, 2 * q_cols + 2 * k_cols), f32),
@@ -697,12 +692,12 @@
             pltpu.VMEM((count, rows, q_cols), bf16),
             pltpu.VMEM((count * rows + 2 * WINDOW, 2 * k_cols), f32),
             pltpu.VMEM((2, count, rows, block_cols), bf16),
-            pltpu.VMEM((k_cols // HEAD, q_cols // k_cols * rows, rows + 2 * WINDOW), f32),
-            pltpu.VMEM((k_cols // HEAD, q_cols // k_cols * rows, LANES), f32),
+            pltpu.VMEM((1 + 2 * (-(-2 * WINDOW // rows)), q_cols // k_cols * rows // 2, rows // 2 + 2 * WINDOW), f32),
             pltpu.VMEM((8, LANES), f32),
             pltpu.VMEM((3, rows, feats), bf16),
             pltpu.VMEM((3, rows, feats), bf16),
-            dma((4,)), dma((3, 2)), dma((3, 2)),
+            pltpu.SMEM((1, sink_logit.shape[0]), f32),
+            dma((7,)), dma((3, 2)), dma((3, 2)),
             dma((2, feats // block_cols)), dma((2, count)),
             dma((2, count)), dma((2, count)), dma((2, count)), dma((2, count)),
             dma((2, 3, count)), dma((3, count)), dma((3, count)), dma((3,)), dma((3,)),
@@ -712,18 +707,22 @@
         ),
         name="layer",
     )(
-        layer_input, output_grad, query_weight, key_weight, value_weight, out_weight,
-        sink_logit.reshape(1, -1),
+        *(
+            pltpu.with_memory_space_constraint(array, pltpu.HBM)
+            for array in (
+                layer_input, output_grad, query_weight, key_weight, value_weight, out_weight,
+                sink_logit.reshape(1, -1),
+            )
+        ),
     )
     kept = [jax.ShapeDtypeStruct(out.shape, out.dtype) for out in outs[:5]]
     stored = pl.pallas_call(
         store_kernel,
         out_shape=(*kept, jax.ShapeDtypeStruct((1, sink_logit.shape[0]), f32)),
-        in_specs=[hbm] * 5 + [vmem],
+        in_specs=[vmem] * 6,
         out_specs=(hbm,) * 5 + (vmem,),
-        scratch_shapes=[pltpu.VMEM(out.shape, out.dtype) for out in kept]
-        + [dma((5,)), dma((5,))],
-        compiler_params=pltpu.CompilerParams(vmem_limit_bytes=VMEM_BYTES),
+        scratch_shapes=[dma((5,))],
+        compiler_params=pltpu.CompilerParams(vmem_limit_bytes=STORE_BYTES),
         name="store",
     )(*outs)
     return tuple(stored[:5]) + (stored[5].reshape(-1),)

time: 86.2 us -> 76.9 us (0.89); the launches traced: 85.1 us -> 76.8 us
  Pallas kernels: 84.3 us -> 76 us
    pallas_call x1, Pallas kernels: 80 us -> 73.7 us  [fused_device(): pl.pallas_call(layer_kernel, out_shape=(jax.ShapeDtypeStruct((rows, feats...]
    pallas_call x1, Pallas kernels: 4.33 us -> 2.32 us  [fused_device(): pl.pallas_call(store_kernel, out_shape=(*kept, jax.ShapeDtypeStruct((1, s...]
where the time goes in v2:
time: 76.9 us; the launch traced here: 76.8 us
  Pallas kernels  76 us (99%)
  between operations  0.8 us (1%)
    pallas_call x1, Pallas kernels, fused_device(): pl.pallas_call(layer_kernel, out_shape=(jax.ShapeDtypeStruct((rows, feats...  73.7 us
    pallas_call x1, Pallas kernels, fused_device(): pl.pallas_call(store_kernel, out_shape=(*kept, jax.ShapeDtypeStruct((1, s...  2.32 us

profile of v2, /device:TPU:0, one launch (start us, length us, event | category | flops | bytes accessed | tf_op | source)
XLA Modules:
  0.0 76.8 jit_solution(4986338938817272343)
XLA Ops:
  0.6 73.7 %layer.1 = (bf16[160,1024]{1,0:T(8,128)(2,1)S(1)}, f32[512,512]{1,0:T(8,128)S(1)}, f32[512,256]{1,0:T(8,128)S(1)}, f32[512,256]{1,0:T(8,128)S(1)}, f32[512,512]{1,0:T(8,128)S(1)}, /*index=5*/f32[8,128]{1,0:T(8,128)S(1)}) custom-call(bf16[160,1024]{1,0:T(8,128)(2,1)} %x_hbm.1, bf16[160,1024]{1,0:T(8,128)(2,1)} %g_hbm.1, bf16[4096,512]{1,0:T(8,128)(2,1)} %wq_hbm.1, ...), custom_call_target="tpu_custom_call" | custom-call | tf_op jit(solution)/shard_map/layer/pallas_call | solution.py:672
  74.3 2.3 %store.1 = (bf16[160,1024]{1,0:T(8,128)(2,1)}, f32[512,512]{1,0:T(8,128)}, f32[512,256]{1,0:T(8,128)}, f32[512,256]{1,0:T(8,128)}, f32[512,512]{1,0:T(8,128)}, /*index=5*/f32[1,4]{1,0:T(1,128)}) custom-call(bf16[160,1024]{1,0:T(8,128)(2,1)S(1)} %get-tuple-element.18.refs_0_, f32[512,512]{1,0:T(8,128)S(1)} %get-tuple-element.19.refs_1_, ...), custom_call_target="tpu_custom_call" | custom-call | tf_op jit(solution)/shard_map/store/pallas_call | solution.py:719

commit v3 on v2

--- a/solution.py
+++ b/solution.py
@@ -258,18 +258,22 @@
     is_across = s // per_slot == across
     is_last = jnp.logical_not(is_home | is_across)
 
-    turn = [(s + d) % count for d in range(count)]
-
-    def column_copy(a, b):
-        span = pl.ds(b * block_cols, block_cols)
-        source, slot = (xg.at[t, 1, :, span], t) if a else (xg.at[across, 0, :, span], across)
+    half = count // 2
+    here_half = s // half * half
+    near = [here_half + i for i in range(half)]
+    far = [half - here_half + i for i in range(half)]
+    sends_near = s // half == t * per_slot // half
+
+    def column_copy(kind, b):
+        a, slot = kind % 2, t if kind else across
         return remote(
-            source, cols.at[a, s], col_send.at[a, b], col_recv.at[a, s], slot * per_slot + b, t
+            xg.at[slot, a, :, pl.ds(b * block_cols, block_cols)], cols.at[a, s],
+            col_send.at[kind, b], col_recv.at[a, s], slot * per_slot + b, t,
         )
 
     def column_arrival(a, source):
         ref = cols.at[a, source]
-        return remote(ref, ref, col_send.at[a, 0], col_recv.at[a, source], turn[1], t)
+        return remote(ref, ref, col_send.at[a, 0], col_recv.at[a, source], (s + 1) % count, t)
 
     def y_copy(a, source):
         ref = cols.at[a, source]
@@ -279,18 +283,20 @@
         ref = cols.at[a, source]
         return remote(ref, ref, chip_send.at[a, source], chip_recv.at[a, source], s, partner)
 
-    def each_column(a, act):
-        slot = t if a else across
+    def each_column(kind, act):
+        slot = t if kind else across
         for b in range(per_slot):
-
-            @pl.when(slot * per_slot + b != s)
+            sent = slot * per_slot + b != s
+
+            @pl.when(sent if kind == 1 else sent & sends_near)
             def _():
-                act(column_copy(a, b))
-
-    def send_columns(a):
-        each_column(a, lambda copy: copy.start())
+                act(column_copy(kind, b))
+
+    def send_columns(kind):
+        each_column(kind, lambda copy: copy.start())
 
     send_columns(1)
+    send_columns(2)
 
     def project_input(slot, first=False):
         cells = xg[slot, 0]
@@ -341,13 +347,10 @@
 
         @pl.when(t * per_slot + b == s)
         def _():
-            cols[1, s] = xg[t, 1, :, span]
-
-        @pl.when(across * per_slot + b == s)
-        def _():
-            cols[0, s] = xg[across, 0, :, span]
-
-    side_first = 1 - x
+            for a in range(2):
+                cols[a, s] = xg[t, a, :, span]
+
+    side_first = 1 - y
 
     def own_rows(block):
         return pl.ds(pl.multiple_of(WINDOW + block * rows, 32), rows)
@@ -381,6 +384,24 @@
         level = z - d * (1 - 2 * way)
         return level, (level >= 0) & (level < depth)
 
+    def crosses(i, level):
+        return (i > 0) | ((level > 0) & (level < depth - 1)) | (level == z)
+
+    def end_copy(way):
+        return z_copy(0, (depth - 1) * way * 2 + (1 - x), way)
+
+    def forward_end(d):
+        for way in range(2):
+            level, there = level_at(d, way)
+
+            @pl.when(there & (level == (depth - 1) * way))
+            def _():
+                end_copy(way).wait_recv()
+
+                @pl.when(goes_on(way))
+                def _():
+                    end_copy(way).start()
+
     def forward(i, d):
         def one(k, _):
             way = lax.rem(side_first + k, 2)
@@ -390,7 +411,10 @@
             def _():
                 block = level * 2 + x
                 z_copy(i, block, way).wait_recv()
-                cross_copy(i, block).start()
+
+                @pl.when(crosses(i, level))
+                def _():
+                    cross_copy(i, block).start()
 
                 @pl.when(goes_on(way))
                 def _():
@@ -413,21 +437,34 @@
     acts[1, s] = acc[:, in_cols:].astype(bf16)
     send_own(2)
 
-    def pass_direct(here, a):
+    straight = [(source, a) for source in near for a in range(2)] + [(source, 1) for source in far]
+    around = [(source, 0) for source in far]
+
+    def pass_direct(here, items):
         @pl.when(here)
         def _():
-            for d, source in enumerate(turn):
-                if d:
+            for source, a in items:
+
+                @pl.when(source != s)
+                def _():
                     column_arrival(a, source).wait_recv()
+
                 y_copy(a, source).start()
                 chip_copy(a, source).start()
 
-    def pass_second(here, a):
+    def pass_second(here, items):
         @pl.when(here)
         def _():
-            for source in turn:
+            for source, a in items:
                 y_copy(a, source).wait_recv()
                 chip_copy(a, source).start()
+
+    def last_arrivals(sources):
+        @pl.when(is_last)
+        def _():
+            for source in sources:
+                for a in range(2):
+                    chip_copy(a, source).wait_recv()
 
     def attend_block(block):
         jobs = [(half_at, kh) for half_at in range(2) for kh in range(key_heads)]
@@ -506,7 +543,14 @@
         cross_copy(i, level * 2 + (1 - x)).wait_recv()
 
     def attend_own():
-        for i in range(3):
+        cross_arrived(0, z)
+        for way in range(2):
+
+            @pl.when(z == (depth - 1) * way)
+            def _():
+                end_copy(way).start()
+
+        for i in range(1, 3):
             cross_arrived(i, z)
 
         @pl.when((z == 0) | (z == depth - 1))
@@ -514,7 +558,7 @@
             block = jnp.where(z == 0, 0, count - 1)
             attend_block(block)
 
-    def attend(d, way, begin=0, end=None):
+    def attend(d, way, span=None):
         level, there = level_at(d, way)
         cross = level * 2 + (1 - x)
         extra = jnp.where(jnp.where(way == 0, level == 0, level == depth - 1), 1, 0)
@@ -531,7 +575,7 @@
             block = jnp.where(inside & passed, block + step, block)
             block = jnp.where(inside & is_end, cross, block)
 
-            @pl.when(k == key_at)
+            @pl.when((k == key_at) & (extra == 0))
             def _():
                 cross_arrived(0, level)
 
@@ -543,24 +587,29 @@
             attend_block(block)
             return 0
 
-        last = stop if end is None else jnp.minimum(stop, end)
-        lax.fori_loop(begin, jnp.where(there, last, begin), one, 0)
+        begin, end = (0, stop) if span is None else span(stop)
+        lax.fori_loop(begin, jnp.where(there, end, begin), one, 0)
 
     def attend_both(d):
-        lax.fori_loop(0, 2, lambda k, _: attend(d, lax.rem(x + k, 2)) or 0, 0)
-
-    pass_direct(is_home, 1)
+        lax.fori_loop(0, 2, lambda k, _: attend(d, k) or 0, 0)
+
+    pass_direct(is_home, straight)
     forward(0, 1)
     forward(1, 1)
     attend_own()
     forward(2, 1)
-    pass_direct(is_across, 0)
+    forward_end(1)
+    pass_direct(is_across, around)
+    is_end = (z == 0) | (z == depth - 1)
+    waits_late = jnp.logical_not(is_end) & ((2 * z < depth) == (y == 1))
+    attend(1, 1 - y, lambda stop: (0, jnp.where(waits_late, stop - 1, 0)))
     forward(0, 2)
     forward(1, 2)
-    attend(1, x)
-    attend(1, 1 - x, 0, 1)
+    attend(1, 1 - y, lambda stop: (jnp.where(waits_late, stop - 1, 0), stop))
+    attend(1, y)
     forward(2, 2)
-    pass_second(is_across, 1)
+    forward_end(2)
+    pass_second(is_across, straight)
     own_dkv = dkv[own_rows(s)]
     own_grads = jnp.concatenate(
         [
@@ -579,60 +628,86 @@
         remote(part.at[i], rs_in.at[i], rs_send.at[i], rs_recv.at[i], s, peer)
         for i, peer in enumerate((partner, partner, across))
     ]
-    for i, slot in enumerate((diag, partner)):
-        part[i] = partial_for(slot).astype(bf16)
-        rs_copies[i].start()
-    far = partial_for(across)
-    rs_copies[0].wait_recv()
-    part[2] = (far + rs_in[0].astype(f32)).astype(bf16)
-    rs_copies[2].start()
-    ig_acc = acc.at[:, :feats]
-    ig_acc[...] = partial_for(t)
-
+    part[0] = partial_for(diag).astype(bf16)
+    rs_copies[0].start()
+    acc[:, :feats] = partial_for(across)
     for d in range(3, depth):
         forward(0, d)
         forward(1, d)
-    attend(1, 1 - x, 1)
-    pass_second(is_home, 0)
-    @pl.when(is_last)
+    def weight_grads(begin, sources, first):
+        last_arrivals(sources)
+        blocks = pl.ds(begin, half)
+        seq = pl.ds(pl.multiple_of(WINDOW + begin * rows, WINDOW), half * rows)
+
+        def flat(value):
+            return value.reshape(half * rows, value.shape[-1])
+
+        left = flat(cols[0, blocks])
+        pieces = (
+            (go_ref, contract_rows(flat(att[blocks]), flat(cols[1, blocks]))),
+            (gq_ref, contract_rows(left, flat(dqs[blocks]))),
+            (gk_ref, contract_rows(left, (dkv[seq, :k_cols] * scaling).astype(bf16))),
+            (gv_ref, contract_rows(left, dkv[seq, k_cols:].astype(bf16))),
+        )
+        for ref, value in pieces:
+            ref[...] = value if first else ref[...] + value
+
+    @pl.when(jnp.logical_not(is_end) & (core == 1))
     def _():
-        for source in range(count):
-            for a in range(2):
-                chip_copy(a, source).wait_recv()
+        weight_grads(here_half, near, True)
+
+    rs_copies[0].wait_recv()
+    part[2] = (acc[:, :feats] + rs_in[0].astype(f32)).astype(bf16)
+    rs_copies[2].start()
+    part[1] = partial_for(partner).astype(bf16)
+    rs_copies[1].start()
+    acc[:, :feats] = partial_for(t)
+
+    @pl.when(jnp.logical_not(is_end) & (core == 0))
+    def _():
+        weight_grads(here_half, near, True)
 
     attend_both(2)
     for d in range(3, depth):
         forward(2, d)
+        forward_end(d)
+    pass_second(is_home, around)
+    @pl.when(is_end)
+    def _():
+        weight_grads(here_half, near, True)
+
+    for d in range(3, depth):
+        attend_both(d)
+    weight_grads(half - here_half, far, False)
+    sg_ref[...] = sinks[...]
     for copy in rs_copies[1:]:
         copy.wait_recv()
     ig_ref[...] = (
-        ig_acc[...] + rs_in[1].astype(f32) + rs_in[2].astype(f32)
+        acc[:, :feats] + rs_in[1].astype(f32) + rs_in[2].astype(f32)
     ).astype(bf16)
-    for d in range(3, depth):
-        attend_both(d)
-    sg_ref[...] = sinks[...]
-    seq = pl.ds(WINDOW, count * rows)
-    left = cols[0].reshape(count * rows, block_cols)
-    go_ref[...] = contract_rows(
-        att[...].reshape(count * rows, q_cols), cols[1].reshape(count * rows, block_cols)
-    )
-    gq_ref[...] = contract_rows(left, dqs[...].reshape(count * rows, q_cols))
-    gk_ref[...] = contract_rows(left, (dkv[seq, :k_cols] * scaling).astype(bf16))
-    gv_ref[...] = contract_rows(left, dkv[seq, k_cols:].astype(bf16))
 
     for copy in to_across + to_partner + relay + rs_copies:
         copy.wait_send()
-    for a in range(2):
-        each_column(a, lambda copy: copy.wait_send())
-        for source in range(count):
-
-            @pl.when(is_home if a else is_across)
-            def _():
+    for kind in range(3):
+        each_column(kind, lambda copy: copy.wait_send())
+    for here, items in ((is_home, straight), (is_across, around)):
+
+        @pl.when(here)
+        def _():
+            for source, a in items:
                 y_copy(a, source).wait_send()
 
-            @pl.when(jnp.logical_not(is_last))
-            def _():
+    @pl.when(jnp.logical_not(is_last))
+    def _():
+        for source in near + far:
+            for a in range(2):
                 chip_copy(a, source).wait_send()
+
+    for way in range(2):
+
+        @pl.when(goes_on(way))
+        def _():
+            end_copy(way).wait_send()
 
     for i in range(3):
         for level in range(depth):
@@ -644,7 +719,9 @@
                 def _():
                     z_copy(i, block, way).wait_send()
 
-            cross_copy(i, block).wait_send()
+            @pl.when(crosses(i, level))
+            def _():
+                cross_copy(i, block).wait_send()
 
 
 def store_kernel(*refs):
@@ -698,7 +775,7 @@
             pltpu.VMEM((3, rows, feats), bf16),
             pltpu.SMEM((1, sink_logit.shape[0]), f32),
             dma((7,)), dma((3, 2)), dma((3, 2)),
-            dma((2, feats // block_cols)), dma((2, count)),
+            dma((3, feats // block_cols)), dma((2, count)),
             dma((2, count)), dma((2, count)), dma((2, count)), dma((2, count)),
             dma((2, 3, count)), dma((3, count)), dma((3, count)), dma((3,)), dma((3,)),
         ],
@@ -730,7 +807,7 @@
 
 def fits_kernel(mesh, layer_width):
     count, tps = mesh.shape["sp"], mesh.shape["tp"]
-    return tps == 4 and count % 8 == 0 and layer_width == count * tps * LANES and HEADS == 2 * KV_HEADS
+    return tps == 4 and count == 8 and layer_width == count * tps * LANES and HEADS == 2 * KV_HEADS
 
 
 def solution(mesh):

time: 76.9 us -> 71.5 us (0.930); the launches traced: 76.8 us -> 70.1 us
  Pallas kernels: 76 us -> 69.3 us
    pallas_call x1, Pallas kernels: 73.7 us -> 67 us  [fused_device(): pl.pallas_call(layer_kernel, out_shape=(jax.ShapeDtypeStruct((rows, feats...]
where the time goes in v3:
time: 71.5 us; the launch traced here: 70.1 us
  Pallas kernels  69.3 us (97%)
  between operations  0.8 us (1%)
    pallas_call x1, Pallas kernels, fused_device(): pl.pallas_call(layer_kernel, out_shape=(jax.ShapeDtypeStruct((rows, feats...  67 us
    pallas_call x1, Pallas kernels, fused_device(): pl.pallas_call(store_kernel, out_shape=(*kept, jax.ShapeDtypeStruct((1, s...  2.32 us

profile of v3, /device:TPU:0, one launch (start us, length us, event | category | flops | bytes accessed | tf_op | source)
XLA Modules:
  0.0 70.1 jit_solution(1608145761511689017)
XLA Ops:
  0.6 67.0 %layer.1 = (bf16[160,1024]{1,0:T(8,128)(2,1)S(1)}, f32[512,512]{1,0:T(8,128)S(1)}, f32[512,256]{1,0:T(8,128)S(1)}, f32[512,256]{1,0:T(8,128)S(1)}, f32[512,512]{1,0:T(8,128)S(1)}, /*index=5*/f32[8,128]{1,0:T(8,128)S(1)}) custom-call(bf16[160,1024]{1,0:T(8,128)(2,1)} %x_hbm.1, bf16[160,1024]{1,0:T(8,128)(2,1)} %g_hbm.1, bf16[4096,512]{1,0:T(8,128)(2,1)} %wq_hbm.1, ...), custom_call_target="tpu_custom_call" | custom-call | tf_op jit(solution)/shard_map/layer/pallas_call | solution.py:749
  67.6 2.3 %store.1 = (bf16[160,1024]{1,0:T(8,128)(2,1)}, f32[512,512]{1,0:T(8,128)}, f32[512,256]{1,0:T(8,128)}, f32[512,256]{1,0:T(8,128)}, f32[512,512]{1,0:T(8,128)}, /*index=5*/f32[1,4]{1,0:T(1,128)}) custom-call(bf16[160,1024]{1,0:T(8,128)(2,1)S(1)} %get-tuple-element.18.refs_0_, f32[512,512]{1,0:T(8,128)S(1)} %get-tuple-element.19.refs_1_, ...), custom_call_target="tpu_custom_call" | custom-call | tf_op jit(solution)/shard_map/store/pallas_call | solution.py:796

commit v4 on v3

--- a/solution.py
+++ b/solution.py
@@ -184,8 +184,8 @@
     x_hbm, g_hbm, wq_hbm, wk_hbm, wv_hbm, wo_hbm, sink_hbm,
     ig_ref, gq_ref, gk_ref, gv_ref, go_ref, sg_ref,
     w_in, wo, xg, acc, kvs, acts, att, dqs, dkv, cols, bias, sinks, part, rs_in, sink_ref,
-    w_sem, ag_send, ag_recv, col_send, col_recv, y_send, y_recv, chip_send, chip_recv,
-    z_sem, cross_sem, acts_recv, rs_send, rs_recv,
+    w_sem, ag_send, ag_recv, col_send, col_recv, y_send, chip_send,
+    z_sem, cross_sem, end_sem, acts_recv, rs_send, rs_recv,
 ):
     bf16, f32 = jnp.bfloat16, jnp.float32
     count, tps = lax.axis_size("sp"), lax.axis_size("tp")
@@ -212,18 +212,18 @@
         )
 
     own = [
-        pltpu.make_async_copy(src, xg.at[t, a], w_sem.at[4 + a])
+        pltpu.make_async_copy(src, xg.at[t, a], w_sem.at[3 + a])
         for a, src in enumerate((x_hbm, g_hbm))
     ]
     for copy in own:
         copy.start()
     weights, at = [], 0
-    for i, src in enumerate((wq_hbm, wk_hbm, wv_hbm)):
+    for src in (wq_hbm, wk_hbm, wv_hbm):
         span = pl.ds(at, src.shape[1])
-        weights.append(pltpu.make_async_copy(src, w_in.at[:, span], w_sem.at[i]))
+        weights.append(pltpu.make_async_copy(src, w_in.at[:, span], w_sem.at[0]))
         at += src.shape[1]
-    weights.append(pltpu.make_async_copy(wo_hbm, wo, w_sem.at[3]))
-    weights.append(pltpu.make_async_copy(sink_hbm, sink_ref, w_sem.at[6]))
+    weights.append(pltpu.make_async_copy(wo_hbm, wo, w_sem.at[1]))
+    weights.append(pltpu.make_async_copy(sink_hbm, sink_ref, w_sem.at[2]))
     for copy in weights:
         copy.start()
 
@@ -240,15 +240,15 @@
     for copy in own:
         copy.wait()
     to_across = [
-        remote(sources[a], xg.at[t, a], ag_send.at[0, a], ag_recv.at[0, a], s, across)
+        remote(sources[a], xg.at[t, a], ag_send.at[0], ag_recv.at[0, a], s, across)
         for a in range(2)
     ]
     to_partner = [
-        remote(sources[a], xg.at[t, a], ag_send.at[1, a], ag_recv.at[1, a], s, partner)
+        remote(sources[a], xg.at[t, a], ag_send.at[1], ag_recv.at[1, a], s, partner)
         for a in range(2)
     ]
     relay = [
-        remote(xg.at[across, a], xg.at[across, a], ag_send.at[2, a], ag_recv.at[2, a], s, partner)
+        remote(xg.at[across, a], xg.at[across, a], ag_send.at[2], ag_recv.at[2, a], s, partner)
         for a in range(2)
     ]
     for copy in to_across + to_partner:
@@ -277,23 +277,23 @@
 
     def y_copy(a, source):
         ref = cols.at[a, source]
-        return remote(ref, ref, y_send.at[a, source], y_recv.at[a, source], s, across)
+        return remote(ref, ref, y_send.at[a], col_recv.at[a, source], s, across)
 
     def chip_copy(a, source):
         ref = cols.at[a, source]
-        return remote(ref, ref, chip_send.at[a, source], chip_recv.at[a, source], s, partner)
-
-    def each_column(kind, act):
+        return remote(ref, ref, chip_send.at[0], col_recv.at[a, source], s, partner)
+
+    def each_column(kind, act, which=None):
         slot = t if kind else across
-        for b in range(per_slot):
+        for b in range(per_slot) if which is None else which:
             sent = slot * per_slot + b != s
 
             @pl.when(sent if kind == 1 else sent & sends_near)
             def _():
                 act(column_copy(kind, b))
 
-    def send_columns(kind):
-        each_column(kind, lambda copy: copy.start())
+    def send_columns(kind, which=None):
+        each_column(kind, lambda copy: copy.start(), which)
 
     send_columns(1)
     send_columns(2)
@@ -328,7 +328,8 @@
         inside = band & (pos >= 0) & (pos < rows * count) if i else band
         bias[i] = jnp.where(inside, 0.0, masked_score)
 
-    for copy in weights:
+    pltpu.make_async_copy(w_in, w_in, w_sem.at[0]).wait()
+    for copy in weights[3:]:
         copy.wait()
     project_input(t, True)
     project_grad(t, True)
@@ -338,7 +339,7 @@
     project_grad(partner)
     to_across[0].wait_recv()
     relay[0].start()
-    send_columns(0)
+    send_columns(0, (0,))
     project_input(across)
     relay[0].wait_recv()
     project_input(diag)
@@ -350,7 +351,6 @@
             for a in range(2):
                 cols[a, s] = xg[t, a, :, span]
 
-    side_first = 1 - y
 
     def own_rows(block):
         return pl.ds(pl.multiple_of(WINDOW + block * rows, 32), rows)
@@ -361,12 +361,12 @@
     def z_copy(i, block, way):
         dev = (z + 1 - 2 * way + depth) % depth * 2 + x
         ref = item(i, block)
-        return remote(ref, ref, z_sem.at[way, i, block], acts_recv.at[i, block], dev, t)
+        return remote(ref, ref, z_sem.at[way, block // 2], acts_recv.at[i, block], dev, t)
 
     def cross_copy(i, block):
         ref = item(i, block)
         return remote(
-            ref, ref, cross_sem.at[i, block], acts_recv.at[i, block], z * 2 + (1 - x), t
+            ref, ref, cross_sem.at[block // 2], acts_recv.at[i, block], z * 2 + (1 - x), t
         )
 
     def goes_on(way):
@@ -385,14 +385,18 @@
         return level, (level >= 0) & (level < depth)
 
     def crosses(i, level):
-        return (i > 0) | ((level > 0) & (level < depth - 1)) | (level == z)
+        return (i < 2) | ((level > 0) & (level < depth - 1)) | (level == z)
 
     def end_copy(way):
-        return z_copy(0, (depth - 1) * way * 2 + (1 - x), way)
-
-    def forward_end(d):
+        block = (depth - 1) * way * 2 + (1 - x)
+        dev = (z + 1 - 2 * way + depth) % depth * 2 + x
+        ref = item(2, block)
+        return remote(ref, ref, end_sem.at[way], acts_recv.at[2, block], dev, t)
+
+    def forward_end(d, allowed=True):
         for way in range(2):
             level, there = level_at(d, way)
+            there = there & allowed
 
             @pl.when(there & (level == (depth - 1) * way))
             def _():
@@ -402,32 +406,33 @@
                 def _():
                     end_copy(way).start()
 
-    def forward(i, d):
-        def one(k, _):
-            way = lax.rem(side_first + k, 2)
-            level, there = level_at(d, way)
-
-            @pl.when(there)
-            def _():
-                block = level * 2 + x
-                z_copy(i, block, way).wait_recv()
-
-                @pl.when(crosses(i, level))
-                def _():
-                    cross_copy(i, block).start()
-
-                @pl.when(goes_on(way))
-                def _():
-                    z_copy(i, block, way).start()
-
-            return 0
-
-        lax.fori_loop(0, 2, one, 0)
+    def forward_way(i, d, way, allowed=True):
+        level, there = level_at(d, way)
+
+        @pl.when(there & allowed)
+        def _():
+            block = level * 2 + x
+            z_copy(i, block, way).wait_recv()
+
+            @pl.when(crosses(i, level))
+            def _():
+                cross_copy(i, block).start()
+
+            @pl.when(goes_on(way))
+            def _():
+                z_copy(i, block, way).start()
+
+    early, late = 1 - y, y
+
+    def forward(i, d, allowed=True):
+        forward_way(i, d, early, allowed)
+        forward_way(i, d, late, allowed)
 
     kvs[own_rows(s)] = acc[:, q_cols:in_cols].astype(bf16)
     send_own(0)
     acts[0, s] = acc[:, :q_cols].astype(bf16)
     send_own(1)
+    send_columns(0, (1,))
 
     to_across[1].wait_recv()
     relay[1].start()
@@ -543,15 +548,13 @@
         cross_copy(i, level * 2 + (1 - x)).wait_recv()
 
     def attend_own():
-        cross_arrived(0, z)
+        for i in range(3):
+            cross_arrived(i, z)
         for way in range(2):
 
             @pl.when(z == (depth - 1) * way)
             def _():
                 end_copy(way).start()
-
-        for i in range(1, 3):
-            cross_arrived(i, z)
 
         @pl.when((z == 0) | (z == depth - 1))
         def _():
@@ -575,13 +578,16 @@
             block = jnp.where(inside & passed, block + step, block)
             block = jnp.where(inside & is_end, cross, block)
 
-            @pl.when((k == key_at) & (extra == 0))
+            @pl.when(k == key_at)
             def _():
                 cross_arrived(0, level)
 
             @pl.when(is_end)
             def _():
                 cross_arrived(1, level)
+
+            @pl.when(is_end & (extra == 0))
+            def _():
                 cross_arrived(2, level)
 
             attend_block(block)
@@ -590,26 +596,38 @@
         begin, end = (0, stop) if span is None else span(stop)
         lax.fori_loop(begin, jnp.where(there, end, begin), one, 0)
 
-    def attend_both(d):
-        lax.fori_loop(0, 2, lambda k, _: attend(d, k) or 0, 0)
-
+    def attend_both(d, span=None):
+        def one(way, _):
+            attend(d, way, None if span is None else functools.partial(span, way))
+            return 0
+
+        lax.fori_loop(0, 2, one, 0)
+
+    is_end = (z == 0) | (z == depth - 1)
+    is_mid = jnp.logical_not(is_end)
+    waits_late = is_mid & ((2 * z < depth) == (y == 1))
+    waits_little = is_mid & jnp.logical_not(waits_late)
     pass_direct(is_home, straight)
-    forward(0, 1)
-    forward(1, 1)
+    forward_way(0, 1, early)
+    forward_way(1, 1, early)
+    forward_way(0, 1, late)
+    forward_way(2, 1, early, is_mid)
+    forward_way(1, 1, late)
     attend_own()
-    forward(2, 1)
+    forward_way(2, 1, early, is_end)
+    forward_way(2, 1, late)
     forward_end(1)
     pass_direct(is_across, around)
-    is_end = (z == 0) | (z == depth - 1)
-    waits_late = jnp.logical_not(is_end) & ((2 * z < depth) == (y == 1))
     attend(1, 1 - y, lambda stop: (0, jnp.where(waits_late, stop - 1, 0)))
     forward(0, 2)
     forward(1, 2)
+    forward(2, 2, waits_little)
+    forward_end(2, waits_little)
     attend(1, 1 - y, lambda stop: (jnp.where(waits_late, stop - 1, 0), stop))
+    pass_second(is_across, straight)
     attend(1, y)
-    forward(2, 2)
-    forward_end(2)
-    pass_second(is_across, straight)
+    forward(2, 2, jnp.logical_not(waits_little))
+    forward_end(2, jnp.logical_not(waits_little))
     own_dkv = dkv[own_rows(s)]
     own_grads = jnp.concatenate(
         [
@@ -631,9 +649,6 @@
     part[0] = partial_for(diag).astype(bf16)
     rs_copies[0].start()
     acc[:, :feats] = partial_for(across)
-    for d in range(3, depth):
-        forward(0, d)
-        forward(1, d)
     def weight_grads(begin, sources, first):
         last_arrivals(sources)
         blocks = pl.ds(begin, half)
@@ -667,17 +682,22 @@
     def _():
         weight_grads(here_half, near, True)
 
+    for d in range(3, depth):
+        forward(0, d)
+        forward(1, d)
     attend_both(2)
+    @pl.when(is_end)
+    def _():
+        weight_grads(here_half, near, True)
+
+    for d in range(3, depth):
+        attend_both(d, lambda way, stop: (0, 1))
     for d in range(3, depth):
         forward(2, d)
         forward_end(d)
     pass_second(is_home, around)
-    @pl.when(is_end)
-    def _():
-        weight_grads(here_half, near, True)
-
     for d in range(3, depth):
-        attend_both(d)
+        attend_both(d, lambda way, stop: (1, stop))
     weight_grads(half - here_half, far, False)
     sg_ref[...] = sinks[...]
     for copy in rs_copies[1:]:
@@ -686,42 +706,52 @@
         acc[:, :feats] + rs_in[1].astype(f32) + rs_in[2].astype(f32)
     ).astype(bf16)
 
-    for copy in to_across + to_partner + relay + rs_copies:
+    def sent(ref, sem):
+        remote(ref, ref, sem, rs_recv.at[0], (s + 1) % count, t).wait_send()
+
+    for i in range(3):
+        sent(xg.at[t], ag_send.at[i])
+    for copy in rs_copies:
         copy.wait_send()
     for kind in range(3):
         each_column(kind, lambda copy: copy.wait_send())
-    for here, items in ((is_home, straight), (is_across, around)):
-
-        @pl.when(here)
-        def _():
-            for source, a in items:
-                y_copy(a, source).wait_send()
+
+    @pl.when(is_home)
+    def _():
+        sent(cols.at[0, pl.ds(here_half, half)], y_send.at[0])
+        sent(cols.at[1], y_send.at[1])
+
+    @pl.when(is_across)
+    def _():
+        sent(cols.at[0, pl.ds(half - here_half, half)], y_send.at[0])
 
     @pl.when(jnp.logical_not(is_last))
     def _():
-        for source in near + far:
-            for a in range(2):
-                chip_copy(a, source).wait_send()
+        sent(cols, chip_send.at[0])
+
+    for level in range(depth):
+        for way in range(2):
+            came = jnp.where(way == 0, level <= z, level >= z)
+
+            @pl.when(came & goes_on(way))
+            def _():
+                sent(acts.at[0, pl.ds(0, 3)], z_sem.at[way, level])
+
+        all_cross = crosses(2, level)
+
+        @pl.when(all_cross)
+        def _():
+            sent(acts.at[0, pl.ds(0, 3)], cross_sem.at[level])
+
+        @pl.when(jnp.logical_not(all_cross))
+        def _():
+            sent(acts.at[0, pl.ds(0, 2)], cross_sem.at[level])
 
     for way in range(2):
 
         @pl.when(goes_on(way))
         def _():
             end_copy(way).wait_send()
-
-    for i in range(3):
-        for level in range(depth):
-            block = level * 2 + x
-            for way in range(2):
-                came = jnp.where(way == 0, level <= z, level >= z)
-
-                @pl.when(came & goes_on(way))
-                def _():
-                    z_copy(i, block, way).wait_send()
-
-            @pl.when(crosses(i, level))
-            def _():
-                cross_copy(i, block).wait_send()
 
 
 def store_kernel(*refs):
@@ -774,10 +804,9 @@
             pltpu.VMEM((3, rows, feats), bf16),
             pltpu.VMEM((3, rows, feats), bf16),
             pltpu.SMEM((1, sink_logit.shape[0]), f32),
-            dma((7,)), dma((3, 2)), dma((3, 2)),
-            dma((3, feats // block_cols)), dma((2, count)),
-            dma((2, count)), dma((2, count)), dma((2, count)), dma((2, count)),
-            dma((2, 3, count)), dma((3, count)), dma((3, count)), dma((3,)), dma((3,)),
+            dma((5,)), dma((3,)), dma((3, 2)),
+            dma((3, feats // block_cols)), dma((2, count)), dma((2,)), dma((1,)),
+            dma((2, count // 2)), dma((count // 2,)), dma((2,)), dma((3, count)), dma((3,)), dma((3,)),
         ],
         compiler_params=pltpu.CompilerParams(
             collective_id=0, has_side_effects=True, vmem_limit_bytes=VMEM_BYTES

time: 71.5 us -> 68.1 us (0.952)
  the two profiles are of different devices: /device:TPU:0 before, /device:TPU:21 now
where the time goes in v4:
time: 68.1 us; the launch traced here: 68 us
  Pallas kernels  67.2 us (99%)
  between operations  0.8 us (1%)
    pallas_call x1, Pallas kernels, fused_device(): pl.pallas_call(layer_kernel, out_shape=(jax.ShapeDtypeStruct((rows, feats...  64.8 us
    pallas_call x1, Pallas kernels, fused_device(): pl.pallas_call(store_kernel, out_shape=(*kept, jax.ShapeDtypeStruct((1, s...  2.32 us

profile of v4, /device:TPU:21, one launch (start us, length us, event | category | flops | bytes accessed | tf_op | source)
XLA Modules:
  0.0 68.0 jit_solution(8182026649156168384)
XLA Ops:
  0.6 64.8 %layer.1 = (bf16[160,1024]{1,0:T(8,128)(2,1)S(1)}, f32[512,512]{1,0:T(8,128)S(1)}, f32[512,256]{1,0:T(8,128)S(1)}, f32[512,256]{1,0:T(8,128)S(1)}, f32[512,512]{1,0:T(8,128)S(1)}, /*index=5*/f32[8,128]{1,0:T(8,128)S(1)}) custom-call(bf16[160,1024]{1,0:T(8,128)(2,1)} %x_hbm.1, bf16[160,1024]{1,0:T(8,128)(2,1)} %g_hbm.1, bf16[4096,512]{1,0:T(8,128)(2,1)} %wq_hbm.1, ...), custom_call_target="tpu_custom_call" | custom-call | tf_op jit(solution)/shard_map/layer/pallas_call | solution.py:779
  65.5 2.3 %store.1 = (bf16[160,1024]{1,0:T(8,128)(2,1)}, f32[512,512]{1,0:T(8,128)}, f32[512,256]{1,0:T(8,128)}, f32[512,256]{1,0:T(8,128)}, f32[512,512]{1,0:T(8,128)}, /*index=5*/f32[1,4]{1,0:T(1,128)}) custom-call(bf16[160,1024]{1,0:T(8,128)(2,1)S(1)} %get-tuple-element.18.refs_0_, f32[512,512]{1,0:T(8,128)S(1)} %get-tuple-element.19.refs_1_, ...), custom_call_target="tpu_custom_call" | custom-call | tf_op jit(solution)/shard_map/store/pallas_call | solution.py:825

commit v5 on v4

--- a/solution.py
+++ b/solution.py
@@ -172,8 +172,8 @@
 LANES = 128
 LOG2E = 1.4426950408889634
 MESH = pl.DeviceIdType.MESH
-VMEM_BYTES = 46 * 1024 * 1024
-STORE_BYTES = 8 * 1024 * 1024
+VMEM_BYTES = 40 * 1024 * 1024
+STORE_BYTES = 12 * 1024 * 1024
 
 
 def dot_nn(a, b):
@@ -182,8 +182,8 @@
 
 def layer_kernel(
     x_hbm, g_hbm, wq_hbm, wk_hbm, wv_hbm, wo_hbm, sink_hbm,
-    ig_ref, gq_ref, gk_ref, gv_ref, go_ref, sg_ref,
-    w_in, wo, xg, acc, kvs, acts, att, dqs, dkv, cols, bias, sinks, part, rs_in, sink_ref,
+    ig_ref, gq_ref, gk_ref, gv_ref, go_ref, sg_ref, att, dqs, dkv, far_cols,
+    w_in, wo, xg, acc, kvs, acts, cols, bias, sinks, part, rs_in, sink_ref,
     w_sem, ag_send, ag_recv, col_send, col_recv, y_send, chip_send,
     z_sem, cross_sem, end_sem, acts_recv, rs_send, rs_recv,
 ):
@@ -618,16 +618,14 @@
     forward_way(2, 1, late)
     forward_end(1)
     pass_direct(is_across, around)
-    attend(1, 1 - y, lambda stop: (0, jnp.where(waits_late, stop - 1, 0)))
+    attend(1, 1 - y, lambda stop: (0, jnp.where(waits_late, stop, 0)))
     forward(0, 2)
     forward(1, 2)
+    attend(1, 1 - y, lambda stop: (jnp.where(waits_late, stop, 0), stop))
     forward(2, 2, waits_little)
     forward_end(2, waits_little)
-    attend(1, 1 - y, lambda stop: (jnp.where(waits_late, stop - 1, 0), stop))
     pass_second(is_across, straight)
     attend(1, y)
-    forward(2, 2, jnp.logical_not(waits_little))
-    forward_end(2, jnp.logical_not(waits_little))
     own_dkv = dkv[own_rows(s)]
     own_grads = jnp.concatenate(
         [
@@ -649,10 +647,12 @@
     part[0] = partial_for(diag).astype(bf16)
     rs_copies[0].start()
     acc[:, :feats] = partial_for(across)
-    def weight_grads(begin, sources, first):
-        last_arrivals(sources)
-        blocks = pl.ds(begin, half)
-        seq = pl.ds(pl.multiple_of(WINDOW + begin * rows, WINDOW), half * rows)
+    forward(2, 2, jnp.logical_not(waits_little))
+    forward_end(2, jnp.logical_not(waits_little))
+    def weight_grads():
+        last_arrivals(near)
+        blocks = pl.ds(here_half, half)
+        seq = pl.ds(pl.multiple_of(WINDOW + here_half * rows, WINDOW), half * rows)
 
         def flat(value):
             return value.reshape(half * rows, value.shape[-1])
@@ -665,11 +665,11 @@
             (gv_ref, contract_rows(left, dkv[seq, k_cols:].astype(bf16))),
         )
         for ref, value in pieces:
-            ref[...] = value if first else ref[...] + value
+            ref[...] = value
 
     @pl.when(jnp.logical_not(is_end) & (core == 1))
     def _():
-        weight_grads(here_half, near, True)
+        weight_grads()
 
     rs_copies[0].wait_recv()
     part[2] = (acc[:, :feats] + rs_in[0].astype(f32)).astype(bf16)
@@ -680,7 +680,7 @@
 
     @pl.when(jnp.logical_not(is_end) & (core == 0))
     def _():
-        weight_grads(here_half, near, True)
+        weight_grads()
 
     for d in range(3, depth):
         forward(0, d)
@@ -688,17 +688,19 @@
     attend_both(2)
     @pl.when(is_end)
     def _():
-        weight_grads(here_half, near, True)
+        weight_grads()
 
     for d in range(3, depth):
         attend_both(d, lambda way, stop: (0, 1))
     for d in range(3, depth):
         forward(2, d)
+        attend_both(d, lambda way, stop: (1, stop - 1))
+    pass_second(is_home, around)
+    last_arrivals(far)
+    far_cols[...] = cols[:, pl.ds(half - here_half, half)]
+    for d in range(3, depth):
         forward_end(d)
-    pass_second(is_home, around)
-    for d in range(3, depth):
-        attend_both(d, lambda way, stop: (1, stop))
-    weight_grads(half - here_half, far, False)
+        attend_both(d, lambda way, stop: (stop - 1, stop))
     sg_ref[...] = sinks[...]
     for copy in rs_copies[1:]:
         copy.wait_recv()
@@ -754,14 +756,40 @@
             end_copy(way).wait_send()
 
 
-def store_kernel(*refs):
-    ins, sink_in, outs, sink_out, sem = refs[:5], refs[5], refs[6:11], refs[11], refs[12]
-    stores = [pltpu.make_async_copy(ins[i], outs[i], sem.at[i]) for i in range(5)]
-    for store in stores:
-        store.start()
+def store_kernel(
+    ig_in, gq_in, gk_in, gv_in, go_in, sink_in, att, dqs, dkv, far_cols,
+    ig_out, gq_out, gk_out, gv_out, go_out, sink_out, gq, gk, gv, go, sem,
+):
+    bf16 = jnp.bfloat16
+    count = lax.axis_size("sp")
+    half = count // 2
+    begin = half - lax.axis_index("sp") // half * half
+    rows = att.shape[1]
+    k_cols = gk.shape[1]
+    blocks = pl.ds(begin, half)
+    seq = pl.ds(pl.multiple_of(WINDOW + begin * rows, WINDOW), half * rows)
+
+    def flat(value):
+        return value.reshape(half * rows, value.shape[-1])
+
+    def send(i, held, out):
+        copy = pltpu.make_async_copy(held, out, sem.at[i])
+        copy.start()
+        return copy
+
+    copies = [send(0, ig_in, ig_out)]
     sink_out[...] = sink_in[0:1, : sink_out.shape[1]]
-    for store in stores:
-        store.wait()
+    left = flat(far_cols[0])
+    go[...] = go_in[...] + contract_rows(flat(att[blocks]), flat(far_cols[1]))
+    copies.append(send(1, go, go_out))
+    gq[...] = gq_in[...] + contract_rows(left, flat(dqs[blocks]))
+    copies.append(send(2, gq, gq_out))
+    gk[...] = gk_in[...] + contract_rows(left, (dkv[seq, :k_cols] * HEAD**-0.5).astype(bf16))
+    copies.append(send(3, gk, gk_out))
+    gv[...] = gv_in[...] + contract_rows(left, dkv[seq, k_cols:].astype(bf16))
+    copies.append(send(4, gv, gv_out))
+    for copy in copies:
+        copy.wait()
 
 
 def fused_device(
@@ -785,9 +813,13 @@
             jax.ShapeDtypeStruct((block_cols, k_cols), f32),
             jax.ShapeDtypeStruct((q_cols, block_cols), f32),
             jax.ShapeDtypeStruct((8, LANES), f32),
+            jax.ShapeDtypeStruct((count, rows, q_cols), bf16),
+            jax.ShapeDtypeStruct((count, rows, q_cols), bf16),
+            jax.ShapeDtypeStruct((count * rows + 2 * WINDOW, 2 * k_cols), f32),
+            jax.ShapeDtypeStruct((2, count // 2, rows, block_cols), bf16),
         ),
         in_specs=[hbm] * 7,
-        out_specs=(vmem,) * 6,
+        out_specs=(vmem,) * 10,
         scratch_shapes=[
             pltpu.VMEM((width, q_cols + 2 * k_cols), bf16),
             pltpu.VMEM(out_weight.shape, bf16),
@@ -795,9 +827,6 @@
             pltpu.VMEM((rows, 2 * q_cols + 2 * k_cols), f32),
             pltpu.VMEM((count * rows + 2 * WINDOW, 2 * k_cols), bf16),
             pltpu.VMEM((2, count, rows, q_cols), bf16),
-            pltpu.VMEM((count, rows, q_cols), bf16),
-            pltpu.VMEM((count, rows, q_cols), bf16),
-            pltpu.VMEM((count * rows + 2 * WINDOW, 2 * k_cols), f32),
             pltpu.VMEM((2, count, rows, block_cols), bf16),
             pltpu.VMEM((1 + 2 * (-(-2 * WINDOW // rows)), q_cols // k_cols * rows // 2, rows // 2 + 2 * WINDOW), f32),
             pltpu.VMEM((8, LANES), f32),
@@ -825,9 +854,9 @@
     stored = pl.pallas_call(
         store_kernel,
         out_shape=(*kept, jax.ShapeDtypeStruct((1, sink_logit.shape[0]), f32)),
-        in_specs=[vmem] * 6,
+        in_specs=[vmem] * 10,
         out_specs=(hbm,) * 5 + (vmem,),
-        scratch_shapes=[dma((5,))],
+        scratch_shapes=[pltpu.VMEM(out.shape, f32) for out in outs[1:5]] + [dma((5,))],
         compiler_params=pltpu.CompilerParams(vmem_limit_bytes=STORE_BYTES),
         name="store",
     )(*outs)

time: 68.1 us -> 67.5 us (level)
  the two profiles are of different devices: /device:TPU:21 before, /device:TPU:3 now
where the time goes in v5:
time: 67.5 us; the launch traced here: 67.4 us
  Pallas kernels  66.6 us (99%)
  between operations  0.8 us (1%)
    pallas_call x1, Pallas kernels, fused_device(): pl.pallas_call(layer_kernel, out_shape=(jax.ShapeDtypeStruct((rows, feats...  63.6 us
    pallas_call x1, Pallas kernels, fused_device(): pl.pallas_call(store_kernel, out_shape=(*kept, jax.ShapeDtypeStruct((1, s...  3.01 us

profile of v5, /device:TPU:3, one launch (start us, length us, event | category | flops | bytes accessed | tf_op | source)
XLA Modules:
  0.0 67.4 jit_solution(9782869797633177269)
XLA Ops:
  0.6 63.6 %layer.1 = (bf16[160,1024]{1,0:T(8,128)(2,1)S(1)}, f32[512,512]{1,0:T(8,128)S(1)}, f32[512,256]{1,0:T(8,128)S(1)}, f32[512,256]{1,0:T(8,128)S(1)}, f32[512,512]{...) custom-call(bf16[160,1024]{1,0:T(8,128)(2,1)} %x_hbm.1, ...), custom_call_target="tpu_custom_call" | custom-call | tf_op jit(solution)/shard_map/layer/pallas_call | solution.py:807
  64.2 3.0 %store.1 = (bf16[160,1024]{1,0:T(8,128)(2,1)}, f32[512,512]{1,0:T(8,128)}, f32[512,256]{1,0:T(8,128)}, f32[512,256]{1,0:T(8,128)}, f32[512,512]{1,0:T(8,128)}, /*index=5*/f32[1,4]{1,0:T(1,128)}) custom-call(bf16[160,1024]{1,0:T(8,128)(2,1)S(1)} %get-tuple-element.22.ig_in, f32[512,512]{1,0:T(8,128)S(1)} %get-tuple-element.23.gq_in, ...), custom_call_target="tpu_custom_call" | custom-call | tf_op jit(solution)/shard_map/store/pallas_call | solution.py:854

commit v6 on v5

--- a/solution.py
+++ b/solution.py
@@ -667,6 +667,8 @@
         for ref, value in pieces:
             ref[...] = value
 
+    for d in range(3, depth):
+        forward(0, d)
     @pl.when(jnp.logical_not(is_end) & (core == 1))
     def _():
         weight_grads()
@@ -683,9 +685,9 @@
         weight_grads()
 
     for d in range(3, depth):
-        forward(0, d)
         forward(1, d)
     attend_both(2)
+    pass_second(is_home, around)
     @pl.when(is_end)
     def _():
         weight_grads()
@@ -695,7 +697,6 @@
     for d in range(3, depth):
         forward(2, d)
         attend_both(d, lambda way, stop: (1, stop - 1))
-    pass_second(is_home, around)
     last_arrivals(far)
     far_cols[...] = cols[:, pl.ds(half - here_half, half)]
     for d in range(3, depth):

time: 67.5 us -> 66.6 us (0.987)
  the two profiles are of different devices: /device:TPU:3 before, /device:TPU:0 now
where the time goes in v6:
time: 66.6 us; the launch traced here: 65.8 us
  Pallas kernels  65 us (98%)
  between operations  0.8 us (1%)
    pallas_call x1, Pallas kernels, fused_device(): pl.pallas_call(layer_kernel, out_shape=(jax.ShapeDtypeStruct((rows, feats...  62 us
    pallas_call x1, Pallas kernels, fused_device(): pl.pallas_call(store_kernel, out_shape=(*kept, jax.ShapeDtypeStruct((1, s...  3.01 us

profile of v6, /device:TPU:0, one launch (start us, length us, event | category | flops | bytes accessed | tf_op | source)
XLA Modules:
  0.0 65.8 jit_solution(347788284624180311)
XLA Ops:
  0.6 62.0 %layer.1 = (bf16[160,1024]{1,0:T(8,128)(2,1)S(1)}, f32[512,512]{1,0:T(8,128)S(1)}, f32[512,256]{1,0:T(8,128)S(1)}, f32[512,256]{1,0:T(8,128)S(1)}, f32[512,512]{...) custom-call(bf16[160,1024]{1,0:T(8,128)(2,1)} %x_hbm.1, ...), custom_call_target="tpu_custom_call" | custom-call | tf_op jit(solution)/shard_map/layer/pallas_call | solution.py:808
  62.7 3.0 %store.1 = (bf16[160,1024]{1,0:T(8,128)(2,1)}, f32[512,512]{1,0:T(8,128)}, f32[512,256]{1,0:T(8,128)}, f32[512,256]{1,0:T(8,128)}, f32[512,512]{1,0:T(8,128)}, /*index=5*/f32[1,4]{1,0:T(1,128)}) custom-call(bf16[160,1024]{1,0:T(8,128)(2,1)S(1)} %get-tuple-element.22.ig_in, f32[512,512]{1,0:T(8,128)S(1)} %get-tuple-element.23.gq_in, ...), custom_call_target="tpu_custom_call" | custom-call | tf_op jit(solution)/shard_map/store/pallas_call | solution.py:855
